TPU v7x, 512 devices: a whole 4x8x8 slice. The times are simulated.
512 devices in a mesh: sp: 32 (over z, x), tp: 16 (over y, core).
Axes of the slice: x: 4, y: 8, z: 8, core: 2. Of those that a mesh axis runs over, the one named last changes fastest.
Arguments:
- tokens: bfloat16 [4096, 2048], P('sp'), may hold values from -6 to 6
- query_narrow: bfloat16 [4096, 2048], P('sp', 'tp'), may hold values from -20 to 20
- key_narrow: bfloat16 [4096, 2048], P('sp', 'tp'), may hold values from -20 to 20
- value_narrow: bfloat16 [4096, 2048], P('sp', 'tp'), may hold values from -6 to 6
- query_broad: bfloat16 [4096, 4096], P('sp', 'tp'), may hold values from -20 to 20
- key_broad: bfloat16 [4096, 4096], P('sp', 'tp'), may hold values from -20 to 20
- value_broad: bfloat16 [4096, 2048], P('sp', 'tp'), may hold values from -6 to 6
- mix_lambda: float32 [2, 16], P(None, 'tp'), may hold values from 0.3 to 0.8
- head_gain: float32 [2, 128], replicated, may hold values from 0.1 to 1.9
- proj_narrow: bfloat16 [2048, 2048], P('tp'), may hold values from -0.09375 to 0.09375
- proj_broad: bfloat16 [2048, 2048], P('tp'), may hold values from -0.09375 to 0.09375
- gain_one: float32 [2048], replicated, may hold values from 0.1 to 1.9
- gain_two: float32 [2048], replicated, may hold values from 0.1 to 1.9
- expert_ids: int32 [4096, 2], P('sp'), may hold values from 0 to 31, all different within a row; in each aligned block of 128 rows (0 to 127, 128 to 255, ...) at most 16 rows name the same one
- expert_gates: float32 [4096, 2], P('sp'), may hold values from 0.1 to 0.9
- gate_weight: bfloat16 [32, 2048, 4096], P('sp', None, 'tp'), may hold values from -0.125 to 0.125
- up_weight: bfloat16 [32, 2048, 4096], P('sp', None, 'tp'), may hold values from -0.125 to 0.125
- down_weight: bfloat16 [32, 4096, 2048], P('sp', 'tp'), may hold values from -0.09375 to 0.09375
Outputs:
- result: bfloat16 [4096, 2048], P('sp')
Inputs may be any that keep to these rules, and one draw needn't show every extreme that they name: `expert_ids`: the 2 experts of a token differ. Among the tokens of one index of sp (aligned blocks of 128 tokens) no expert is named by more than 16 tokens, and in some blocks one expert is named by exactly 16.
All inputs are finite; a program needn't handle non-finite values.
Results may differ from a plain program's by a relative error of at most 0.015.
Values may be sent and summed in bfloat16 or wider, within the bound.
A program may use at most 64 MiB of HBM per device.

v0:
```python
import jax
import jax.numpy as jnp
from jax import lax
from jax.sharding import Mesh
from jax.sharding import PartitionSpec as P

QK_NARROW = 64
QK_BROAD = 128
V = 128
TOP = 2
CAP = 16
TP = ("tp_0", "tp_1")


deep_alpha = 8.0**0.25
norm_eps = 1e-05


def in_one_piece(arrays, axis, dim, along):
    ends, at = ([], 0)
    for a in arrays[:-1]:
        at += a.shape[along]
        ends.append(at)
    both = jnp.concatenate(arrays, axis=along)
    return tuple(jnp.split(lax.all_gather(both, axis, axis=dim, tiled=True), ends, axis=along))


def cut_along(value, dim, size):
    before, after = (value.shape[:dim], value.shape[dim + 1 :])
    return jnp.moveaxis(value.reshape(*before, size, -1, *after), dim, 0)


def sum_at_owner(value, axis, dim):
    size = lax.axis_size(axis)
    pieces = lax.all_to_all(cut_along(value, dim, size), axis, 0, 0, tiled=True)
    return jnp.sum(pieces.astype(jnp.float32), axis=0)


def copy_for_each(value, axis):
    copies = jnp.broadcast_to(value, (lax.axis_size(axis), *value.shape))
    return lax.all_to_all(copies, axis, split_axis=0, concat_axis=0, tiled=True)


def laid_out(pieces, dim):
    dims = list(pieces.shape[1:])
    dims[dim] *= pieces.shape[0]
    return jnp.moveaxis(pieces, 0, dim).reshape(dims)


def gathered_copies(value, axis, dim):
    pieces = copy_for_each(value, axis)
    return laid_out(pieces, dim)


def gather_axes(value, axes, dim):
    for axis in reversed(axes):
        value = lax.all_gather(value, axis, axis=dim, tiled=True)
    return value


def layer_scale(inputs, gains):
    center = jnp.mean(inputs, -1, keepdims=True)
    spread = jnp.mean(jnp.square(inputs - center), -1, keepdims=True)
    return (inputs - center) * lax.rsqrt(spread + norm_eps) * gains


def head_fold(running, queries, key_rows, values, key_width):
    maxima, totals, weighted = running
    length = key_rows.shape[0]
    head_count = queries.shape[1]
    keyed = key_rows.reshape(length, head_count, 2, key_width)
    valued = values.reshape(length, head_count, V)
    scores = jnp.einsum(
        "qhmd,khmd->hmqk", queries, keyed, preferred_element_type=jnp.float32
    ) * key_width ** (-0.5)
    updated = jnp.maximum(maxima, jnp.max(scores, -1))
    exponent = jnp.exp(scores - updated[..., None])
    totals = jnp.sum(exponent, -1)
    weighted = jnp.einsum(
        "hmqk,khv->hmqv", exponent.astype(jnp.bfloat16), valued, preferred_element_type=jnp.float32
    )
    return (updated, totals, weighted)


def head_output(running, mixing, gains):
    maxima, totals, weighted = running
    diff = (
        weighted[:, 0] / totals[:, 0, :, None]
        - mixing[:, None, None] * weighted[:, 1] / totals[:, 1, :, None]
    )
    normed = (diff * lax.rsqrt(jnp.mean(diff * diff, -1, keepdims=True) + norm_eps) * gains).astype(
        jnp.bfloat16
    )
    return jnp.moveaxis(normed, 0, 1).reshape(normed.shape[1], -1)


def on_device(
    tokens,
    query_narrow,
    key_narrow,
    value_narrow,
    query_broad,
    key_broad,
    value_broad,
    mix_lambda,
    head_gain,
    proj_narrow,
    proj_broad,
    gain_one,
    gain_two,
    expert_ids,
    expert_gates,
    gate_weight,
    up_weight,
    down_weight,
):
    token_count = tokens.shape[0]
    model_width = tokens.shape[1]
    head_count = value_narrow.shape[1] // V
    queries_first = query_narrow.reshape(token_count, head_count, 2, QK_NARROW)
    queries_second = query_broad.reshape(token_count, head_count, 2, QK_BROAD)
    start_state = (
        jnp.full((head_count, 2, token_count), -1e30, jnp.float32),
        jnp.zeros((head_count, 2, token_count), jnp.float32),
        jnp.zeros((head_count, 2, token_count, V), jnp.float32),
    )
    pieces = in_one_piece((key_narrow, value_narrow, key_broad, value_broad), "sp", 0, 1)
    state_first = head_fold(start_state, queries_first, pieces[0], pieces[1], QK_NARROW)
    state_second = head_fold(start_state, queries_second, pieces[2], pieces[3], QK_BROAD)
    heads_first = head_output(state_first, mix_lambda[0], head_gain[0])
    heads_second = head_output(state_second, mix_lambda[1], head_gain[1])
    tp_count = lax.axis_size(TP)
    row_share = token_count // tp_count
    partial_value = jnp.dot(heads_first, proj_narrow, preferred_element_type=jnp.float32)
    partial_value = partial_value + jnp.dot(
        heads_second, proj_broad, preferred_element_type=jnp.float32
    )
    attn = sum_at_owner(
        partial_value.astype(jnp.bfloat16).astype(jnp.float32).astype(jnp.bfloat16), TP, 0
    )
    own_tokens = lax.dynamic_slice_in_dim(tokens, lax.axis_index(TP) * row_share, row_share, 0)
    normed_share = layer_scale(deep_alpha * own_tokens.astype(jnp.float32) + attn, gain_one).astype(
        jnp.bfloat16
    )
    mixed_rows = gathered_copies(normed_share, TP, 0)
    sp_count = lax.axis_size("sp")
    local_experts = gate_weight.shape[0]
    experts_all = local_experts * sp_count
    chosen = expert_ids.reshape(-1)
    onehot = (chosen[:, None] == jnp.arange(experts_all, dtype=jnp.int32)[None, :]).astype(
        jnp.int32
    )
    before = jnp.cumsum(onehot, axis=0, dtype=jnp.int32) - onehot
    slot_index = jnp.sum(before * onehot, axis=-1, dtype=jnp.int32)
    position = slot_index * experts_all + chosen
    repeated = jnp.repeat(mixed_rows, TOP, axis=0)
    outgoing = jnp.zeros((CAP * experts_all, model_width), jnp.bfloat16).at[position].set(repeated)
    outgoing = outgoing.reshape(CAP, experts_all, model_width)
    slot_share = CAP // tp_count
    arrived = lax.all_to_all(outgoing, "sp", split_axis=1, concat_axis=1, tiled=True)
    expert_rows = arrived.reshape(CAP * sp_count, local_experts, model_width)
    gated = jnp.einsum("rxd,xdf->rxf", expert_rows, gate_weight, preferred_element_type=jnp.float32)
    lifted = jnp.einsum("rxd,xdf->rxf", expert_rows, up_weight, preferred_element_type=jnp.float32)
    activated = (jax.nn.silu(gated) * lifted).astype(jnp.bfloat16)
    product = jnp.einsum("rxf,xfd->rxd", activated, down_weight, preferred_element_type=jnp.float32)
    summed = sum_at_owner(
        product.astype(jnp.bfloat16).astype(jnp.float32).astype(jnp.bfloat16), TP, 0
    )
    returning = summed.astype(jnp.bfloat16).reshape(
        slot_share, sp_count, local_experts, model_width
    )
    returned = lax.all_to_all(returning, "sp", split_axis=1, concat_axis=1, tiled=True)
    collected = gather_axes(returned, TP, 0)
    picked = collected.reshape(CAP * experts_all, model_width)[position].reshape(
        token_count, TOP, model_width
    )
    routed = jnp.sum(expert_gates[:, :, None] * picked.astype(jnp.float32), axis=1)
    return layer_scale(deep_alpha * mixed_rows.astype(jnp.float32) + routed, gain_two).astype(
        jnp.bfloat16
    )


def solution(mesh):
    finer = Mesh(mesh.devices.reshape(mesh.shape["sp"], 8, 2), ("sp", "tp_0", "tp_1"))
    return jax.shard_map(
        on_device,
        mesh=finer,
        in_specs=(
            P("sp", None),
            P("sp", TP),
            P("sp", TP),
            P("sp", TP),
            P("sp", TP),
            P("sp", TP),
            P("sp", TP),
            P(None, TP),
            P(),
            P(TP, None),
            P(TP, None),
            P(),
            P(),
            P("sp", None),
            P("sp", None),
            P("sp", None, TP),
            P("sp", None, TP),
            P("sp", TP, None),
        ),
        out_specs=P("sp", None),
        check_vma=False,
    )
```

profile of v0, /device:TPU:1, one launch (start us, length us, event | category | flops | bytes accessed | tf_op | source)
XLA Modules:
  0.0 375.7 jit_solution(16029199645535660946)
XLA Ops:
  6.5 1.0 copy.61
  11.8 1.4 fusion.71
  13.9 92.7 %all-gather.3.cloned.1.call-done = bf16[4096,640]{0,1:T(8,128)(2,1)} async-done(((bf16[128,640]{0,1:T(8,128)(2,1)}), bf16[4096,640]{0,1:T(8,128)(2,1)}) %all-gather.3.cloned.1.call-update) | async-done | bytes 5242896 | tf_op jit(solution)/shard_map/all_gather | solution.py:25
  106.6 1.2 slice-done.2
  107.8 0.9 fusion.72
  111.2 1.6 slice-done.3
  112.8 1.0 fusion.73
  116.0 1.0 fusion.53
  117.1 1.8 fusion.7
  118.9 10.2 %all-to-all-start = ((bf16[16,8,2048]{2,1,0:T(8,128)(2,1)}), bf16[16,8,2048]{2,1,0:T(8,128)(2,1)S(1)}, u32[]{:S(2)}, u32[]{:S(2)}) async-start(bf16[16,8,2048]{2,1,0:T(8,128)(2,1)} %fusion.7), calls=%async_computation | async-start | bytes 1048576 | tf_op jit(solution)/shard_map/all_to_all | solution.py:35
  129.1 17.2 %all-to-all-done = bf16[16,8,2048]{2,1,0:T(8,128)(2,1)S(1)} async-done(((bf16[16,8,2048]{2,1,0:T(8,128)(2,1)}), bf16[16,8,2048]{2,1,0:T(8,128)(2,1)S(1)}, u32[]{:S(2)}, u32[]{:S(2)}) %all-to-all-start) | async-done | bytes 524320 | tf_op jit(solution)/shard_map/all_to_all | solution.py:35
  146.4 0.9 fusion.69
  147.3 1.0 multiply_reduce_fusion.2
  150.0 3.5 all-to-all-start.1
  155.0 15.1 %all-to-all-done.1 = bf16[16,8,2048]{2,1,0:T(8,128)(2,1)S(1)} async-done(((bf16[16,8,2048]{2,1,0:T(8,128)(2,1)}), bf16[16,8,2048]{2,1,0:T(8,128)(2,1)S(1)}, u32[]{:S(2)}, u32[]{:S(2)}) %all-to-all-start.1) | async-done | bytes 524320 | tf_op jit(solution)/shard_map/all_to_all | solution.py:41
  170.8 1.2 reshape.551
  172.0 4.4 %scatter_custom_fusion = bf16[512,2048]{1,0:T(8,128)(2,1)} fusion(s32[256]{0:T(256)S(1)} %bitcast.209, bf16[256,2048]{1,0:T(8,128)(2,1)} %reshape.551, bf16[]{:T(256)} %constant.55.clone.1), kind=kCustom, calls=%fused_computation.36 | custom fusion | bytes 2097664 | tf_op jit(solution)/shard_map/scatter | solution.py:157
  176.4 2.7 copy.73
  179.2 59.9 %all_to_all.25 = bf16[16,32,2048]{2,0,1:T(8,128)(2,1)S(1)} all-to-all(bf16[16,32,2048]{2,0,1:T(8,128)(2,1)S(1)} %copy.73), channel_id=1, replica_groups=mesh['sp'=32,'tp_0'=8,'tp_1'=2] {'sp'}, dimensions={1} | all-to-all | bytes 4194304 | tf_op jit(solution)/shard_map/all_to_all | solution.py:160
  239.1 1.2 copy.74
  240.3 1.3 copy-done.1
  242.3 5.5 %convolution_convert_fusion = bf16[512,2048]{1,0:T(8,128)(2,1)} fusion(bf16[512,2048]{1,0:T(8,128)(2,1)} %bitcast.203, bf16[1,256,2048]{2,1,0:T(8,128)(2,1)S(1)} %copy-done, bf16[1,2048,256]{2,1,0:T(8,128)(2,1)} %param.34, f32[512,1,256]{2,0,1:T(8,128)S(1)} %convolution_bitcast_fusion.1), kind=kOutput, calls=%fused_computation.12 | convolution fusion | flops 1075576832 | bytes 6815744 | tf_op jit(solution)/shard_map/rxf,xfd->rxd/dot_general | solution.py:165
  247.8 55.7 %all_to_all.26 = bf16[16,32,1,2048]{3,1,2,0:T(8,128)(2,1)} all-to-all(bf16[16,32,1,2048]{3,1,2,0:T(8,128)(2,1)} %bitcast.204), channel_id=1, replica_groups=mesh['sp'=32,'tp_0'=8,'tp_1'=2] {'tp_0','tp_1'}, dimensions={0} | all-to-all | bytes 4194304 | tf_op jit(solution)/shard_map/all_to_all | solution.py:35
  303.5 2.0 reduce_sum.127
  306.2 1.4 reduce.16
  307.7 15.3 %all_to_all.27 = bf16[32,2,1024]{2,1,0:T(2,128)(2,1)S(1)} all-to-all(bf16[32,2,1024]{2,1,0:T(2,128)(2,1)S(1)} %reshape.560), channel_id=1, replica_groups=mesh['sp'=32,'tp_0'=8,'tp_1'=2] {'sp'}, dimensions={0} | all-to-all | bytes 262144 | tf_op jit(solution)/shard_map/all_to_all | solution.py:172
  323.2 2.3 all_gather.10
  325.7 30.0 %all-gather.5.cloned.1.call-done = bf16[16,32,1,2048]{3,1,2,0:T(8,128)(2,1)} async-done(((bf16[2,32,1,2048]{3,1,2,0:T(8,128)(2,1)}), bf16[16,32,1,2048]{3,1,2,0:T(8,128)(2,1)}) %all-gather.5.cloned.1.call-update) | async-done | bytes 2097168 | tf_op jit(solution)/shard_map/all_gather | solution.py:57
  355.7 4.2 %gather_fusion = bf16[256,2048]{1,0:T(8,128)(2,1)S(1)} fusion(bf16[512,2048]{1,0:T(8,128)(2,1)} %bitcast.195, s32[1024]{0:T(1024)S(1)} %pad_clamp_fusion), kind=kCustom, calls=%fused_computation | custom fusion | bytes 2098176 | tf_op jit(solution)/shard_map/gather | solution.py:174
  359.9 2.4 reshape.538
  362.3 4.7 %multiply_reduce_fusion = f32[128,2048]{1,0:T(8,128)S(1)} fusion(f32[128,2,2048]{2,1,0:T(2,128)} %reshape.538, f32[128,2]{1,0:T(8,128)S(1)} %copy.68), kind=kLoop, calls=%fused_computation.18 | loop fusion | flops 786432 | bytes 3146752 | tf_op jit(solution)/shard_map/reduce_sum | solution.py:177
  367.8 1.1 multiply_convert_fusion
  (80 shorter events, 16.0 us)
Async XLA Ops:
  6.5 235.7 %copy-start = (bf16[1,256,2048]{2,1,0:T(8,128)(2,1)S(1)}, bf16[1,256,2048]{2,1,0:T(8,128)(2,1)}, u32[]{:S(2)}) copy-start(bf16[1,256,2048]{2,1,0:T(8,128)(2,1)} %param.35) | copy-start | bytes 3145732
  6.5 100.1 %all-gather.3.cloned.1.call-start = ((), (), s32[]{:S(2)}) async-start(), calls=%async_computation.5 | async-start | bytes 5406720 | tf_op jit(solution)/shard_map/all_gather | solution.py:25
  106.6 1.2 slice-start.2
  106.6 2.8 slice-start
  107.8 1.8 slice-start.1
  111.2 1.6 slice-start.3
  111.2 1.6 copy-start.4
  114.4 1.6 copy-start.2
  115.3 1.8 copy-start.3
  117.1 31.2 %copy-start.6 = (f32[2048]{0:T(1024)S(1)}, f32[2048]{0:T(1024)}, u32[]{:S(2)}) copy-start(f32[2048]{0:T(1024)} %param.29) | copy-start | bytes 24580
  118.9 34.6 %copy-start.7 = (s32[128,2]{0,1:T(2,128)S(1)}, s32[128,2]{0,1:T(2,128)}, u32[]{:S(2)}) copy-start(s32[128,2]{0,1:T(2,128)} %param.31) | copy-start | bytes 3076
  118.9 27.4 %all-to-all-start = ((bf16[16,8,2048]{2,1,0:T(8,128)(2,1)}), bf16[16,8,2048]{2,1,0:T(8,128)(2,1)S(1)}, u32[]{:S(2)}, u32[]{:S(2)}) async-start(bf16[16,8,2048]{2,1,0:T(8,128)(2,1)} %fusion.7), calls=%async_computation | async-start | bytes 1048576 | tf_op jit(solution)/shard_map/all_to_all | solution.py:35
  150.0 20.2 %all-to-all-start.1 = ((bf16[16,8,2048]{2,1,0:T(8,128)(2,1)}), bf16[16,8,2048]{2,1,0:T(8,128)(2,1)S(1)}, u32[]{:S(2)}, u32[]{:S(2)}) async-start(bf16[16,8,2048]{2,1,0:T(8,128)(2,1)} %broadcast_in_dim.9), calls=%async_computation.1 | async-start | bytes 1048576 | tf_op jit(solution)/shard_map/all_to_all | solution.py:41
  153.4 202.2 %all-gather.5.cloned.1.call-start = ((), (), s32[]{:S(2)}) async-start(), calls=%async_computation.6 | async-start | bytes 2359296 | tf_op jit(solution)/shard_map/all_gather | solution.py:57
  239.1 2.5 copy-start.9
  240.2 1.3 copy-start.1
  303.5 22.1 %copy-start.8 = (f32[128,2]{0,1:T(2,128)S(1)}, f32[128,2]{0,1:T(2,128)}, u32[]{:S(2)}) copy-start(f32[128,2]{0,1:T(2,128)} %param.32) | copy-start | bytes 3076
  367.0 0.7 copy-start.5
Sparse Core Ops, SparseCore 0:
  11.0 95.5 all-gather.2
  325.7 29.9 all-gather.4
where the time goes:
time: 380 us; the launch traced here: 376 us
  waiting for transfers between devices  155 us (41%)
  blocking collectives  133 us (35%)
  local copies, waits for them, and re-layouts  30.6 us (8%)
  other arithmetic  16.5 us (4%)
  starting transfers between devices  13.7 us (4%)
  between operations  13.7 us (4%)
  matrix products  12.8 us (3%)
    all_gather x1, waiting for transfers between devices, in_one_piece(): lax.all_gather(both, axis, axis=dim, tiled=True)  92.7 us
    all_to_all x1, blocking collectives, on_device(): lax.all_to_all(outgoing, 'sp', split_axis=1, concat_axis=1, tiled=True)  59.9 us
    all_to_all x1, blocking collectives, sum_at_owner(): pieces = lax.all_to_all(cut_along(value, dim, size), axis, 0, 0, tiled=True)  55.7 us
    all_gather x1, waiting for transfers between devices, gather_axes(): value = lax.all_gather(value, axis, axis=dim, tiled=True)  30 us
    all_to_all x1, waiting for transfers between devices, sum_at_owner(): pieces = lax.all_to_all(cut_along(value, dim, size), axis, 0, 0, tiled=True)  17.2 us
    all_to_all x1, blocking collectives, on_device(): lax.all_to_all(returning, 'sp', split_axis=1, concat_axis=1, tiled=True)  15.3 us
    all_to_all x1, waiting for transfers between devices, copy_for_each(): return lax.all_to_all(copies, axis, split_axis=0, concat_axis=0, tiled=True)  15.1 us
    all_to_all x1, starting transfers between devices, sum_at_owner(): pieces = lax.all_to_all(cut_along(value, dim, size), axis, 0, 0, tiled=True)  10.2 us
  transfers between devices with their start and end apart: 4, of which 4 were waited for; matrix products, arithmetic and copies ran while one was open for 1% of the time, Pallas kernels for 0%

commit v1 on v0

v1 whole, which is shorter than its diff:
```python
import functools

import jax
import jax.numpy as jnp
from jax import lax
from jax.experimental import pallas as pl
from jax.experimental.pallas import tpu as pltpu
from jax.sharding import Mesh
from jax.sharding import PartitionSpec as P

MESH = pl.DeviceIdType.MESH
NZ, NX, NY = 8, 4, 8
NSP = NZ * NX
CAP = 16
F32, BF16 = jnp.float32, jnp.bfloat16
ALPHA = 8.0**0.25
EPS = 1e-05
LOG2E = 1.4426950408889634
SCALES = (64**-0.5 * LOG2E, 128**-0.5 * LOG2E)


def dot(a, b, ca, cb):
    return lax.dot_general(a, b, (((ca,), (cb,)), ((), ())), preferred_element_type=F32)


def wait(ref, sem):
    pltpu.make_async_copy(ref, ref, sem).wait()


def send(src, dst, send_sem, recv_sem, dev):
    pltpu.make_async_remote_copy(
        src_ref=src, dst_ref=dst, send_sem=send_sem, recv_sem=recv_sem, device_id=dev, device_id_type=MESH
    ).start()


def row_iota(shape):
    return lax.broadcasted_iota(jnp.int32, shape, 0)


def lane_iota(shape):
    return lax.broadcasted_iota(jnp.int32, shape, 1)


def kernel(
    lam, ids, gates, hgain, g1, g2, tok, qn, kn, vn, qb, kb, vb, pn, pb, gw, uw, dw,
    out,
    kv, qraw, qs, acc, ml, osend, orecv, ssend, srecv, wp, wpt, tokraw, tokt, rows, cols, dmat, pmat,
    heads, rsend, rrecv, stat1, mixed, disp, xg, wg, wu, wd, accg, accu, act, part, dsend, drecv,
    ret, eo, fin, stat2, outb,
    loc, kvs, kvr, qsd, qrv, wsd, wrv, osd, orv, ssd, srv, hsd, hrv, rsd, rrv, s1s, s1r, dps, dpr,
    xgs, xgr, dds, ddr, rts, rtr, fns, fnr, s2s, s2r, oud,
):
    z, x, y, c = (lax.axis_index(n) for n in ("z", "x", "y", "c"))
    me = z * NX + x
    own = 2 * y + c
    other = 1 - c
    half = me // 16
    zp, zm = lax.rem(z + 1, NZ), lax.rem(z + NZ - 1, NZ)
    yp, ym = lax.rem(y + 1, NY), lax.rem(y + NY - 1, NY)
    partner = (z, x, y, other)

    def col(j):
        return pl.ds(pl.multiple_of(j * 128, 128), 128)

    def local(i, src, dst):
        cp = pltpu.make_async_copy(src, dst, loc.at[i])
        cp.start()
        return cp

    first = [
        local(0, kn, kv.at[0, 0]), local(1, vn, kv.at[0, 1]),
        local(2, kb.at[:, pl.ds(0, 128)], kv.at[0, 2]), local(3, kb.at[:, pl.ds(128, 128)], kv.at[0, 3]),
        local(4, vb, kv.at[0, 4]),
        local(5, qn, qraw.at[0, 0]), local(6, qb.at[:, pl.ds(0, 128)], qraw.at[0, 1]),
        local(7, qb.at[:, pl.ds(128, 128)], qraw.at[0, 2]),
    ]
    tokcp = local(8, tok.at[:, col(own)], tokraw)

    barrier = pltpu.get_barrier_semaphore()

    def greet(j, carry):
        t = lax.rem(me + j, NSP)
        for cc in (c, other):
            pl.semaphore_signal(barrier, inc=1, device_id=(t // NX, lax.rem(t, NX), y, cc), device_id_type=MESH)
        return carry

    lax.fori_loop(1, NSP, greet, 0)
    for dy in range(NY):
        for dc in range(2):
            if dy or dc:
                pl.semaphore_signal(
                    barrier, inc=1, device_id=(z, x, lax.rem(y + dy, NY), c if dc == 0 else other), device_id_type=MESH
                )
    pl.semaphore_wait(barrier, 2 * (NSP - 1) + 2 * NY - 1)

    for cp in first:
        cp.wait()
    N, B = pl.ds(0, 2), pl.ds(2, 3)

    def kv_send(d, step, piece, src_slot, dst_slot):
        part_of = (N, B)[piece]
        send(
            kv.at[src_slot, part_of], kv.at[dst_slot, part_of], kvs.at[d, step, piece], kvr.at[dst_slot, piece],
            ((zp, zm)[d], x, y, c),
        )

    def kv_wait(slot, piece):
        wait(kv.at[slot, (N, B)[piece]], kvr.at[slot, piece])

    for piece in (0, 1):
        kv_send(0, 0, piece, 0, 1)
        kv_send(1, 0, piece, 0, 5)
    for r in (2, 1, 3):
        send(qraw.at[0], qraw.at[r], qsd.at[r - 1], qrv.at[r - 1], (z, lax.rem(x + NX - r, NX), y, c))

    def proj(j, carry):
        for k, w in enumerate((pn, pb)):
            dst = pl.ds(k * 128, 128)
            pltpu.make_async_copy(w.at[:, col(2 * j + c)], wp.at[0, j, dst], loc.at[9]).start()
            send(w.at[:, col(2 * j + other)], wp.at[1, j, dst], wsd.at[0], wrv.at[0], partner)
        return carry

    lax.fori_loop(0, NY, proj, 0)
    for k, (w, buf) in enumerate(((gw, wg), (uw, wu), (dw, wd))):
        local(10 + k, w.at[0], buf.at[0])
        send(w.at[0], buf.at[1], wsd.at[1 + k], wrv.at[1 + k], partner)

    lane = lane_iota((128, 128))
    sub = row_iota((128, 128))
    idf = ids[...].astype(F32)
    gat = gates[...]
    table = jnp.where(lane == 0, idf[:, 0:1], jnp.where(lane == 1, idf[:, 1:2], 0.0))
    idr = table.T
    rows_e = row_iota((NSP, 128)).astype(F32)
    hot = [(idr[k : k + 1, :] == rows_e).astype(F32) for k in range(2)]
    upper = (sub < lane).astype(F32).astype(BF16)
    before = dot((hot[0] + hot[1]).astype(BF16), upper, 1, 0)
    pos = [
        idr[k : k + 1, :] * float(CAP) + jnp.sum(before * hot[k], axis=0, keepdims=True) for k in range(2)
    ]
    rows_s = row_iota((CAP * NSP, 128)).astype(F32)
    dmat[...] = ((pos[0] == rows_s).astype(F32) + (pos[1] == rows_s).astype(F32)).astype(BF16)
    posc = jnp.where(sub == 0, pos[0], jnp.where(sub == 1, pos[1], 0.0)).T
    lanes_s = lane_iota((128, CAP * NSP)).astype(F32)
    for k in range(2):
        pmat[k] = (posc[:, k : k + 1] == lanes_s).astype(F32).astype(BF16)
    gain_rows = jnp.where(
        sub == 0, hgain[0:1, :], jnp.where(sub == 1, hgain[1:2, :], jnp.where(sub == 2, g1[pl.ds(own, 1), :], 0.0))
    )
    cols[...] = gain_rows.T
    tokcp.wait()
    tokt[...] = tokraw[...].astype(F32).T

    for r in (1, 3, 2):
        wait(qraw.at[r], qrv.at[r - 1])
    low = lane < 64
    for r in range(NX):
        at = pl.ds(r * 128, 128)
        narrow = qraw[r, 0]
        qs[0, at, :] = jnp.where(low, narrow, jnp.zeros_like(narrow))
        qs[1, at, :] = jnp.where(low, jnp.zeros_like(narrow), narrow)
        qs[2, at, :] = qraw[r, 1]
        qs[3, at, :] = qraw[r, 2]

    def attend(group, slots, start):
        def one_map(i, carry):
            m = group * 2 + i
            k_at = 0 if group == 0 else 2 + i
            v_at = 1 if group == 0 else 4
            query = qs[m]
            scores = [dot(kv[s, k_at], query, 1, 1) for s in slots]
            top = functools.reduce(jnp.maximum, [jnp.max(s, axis=0, keepdims=True) for s in scores])
            if not start:
                old = ml[pl.ds(m, 1), :]
                top = jnp.maximum(old, top)
            expo = [jnp.exp2((s - top) * SCALES[group]) for s in scores]
            total = functools.reduce(jnp.add, [jnp.sum(e, axis=0, keepdims=True) for e in expo])
            numer = functools.reduce(
                jnp.add, [dot(kv[s, v_at], e.astype(BF16), 0, 0) for s, e in zip(slots, expo)]
            )
            if start:
                acc[m] = numer
                ml[pl.ds(4 + m, 1), :] = total
            else:
                shrink = jnp.exp2((old - top) * SCALES[group])
                acc[m] = acc[m] * shrink + numer
                ml[pl.ds(4 + m, 1), :] = ml[pl.ds(4 + m, 1), :] * shrink + total
            ml[pl.ds(m, 1), :] = top
            return carry

        lax.fori_loop(0, 2, one_map, 0)

    def arrive(d, piece):
        kv_wait(d, piece)
        if d < 3 or piece == 0:
            kv_send(0, d, piece, d, d + 1)
        kv_wait(4 + d, piece)
        if d < 3:
            kv_send(1, d, piece, 4 + d, 5 + d)
        elif piece == 1:
            kv_send(1, d, piece, 7, 4)

    arrive(1, 0)
    attend(0, (0,), True)
    arrive(1, 1)
    attend(1, (0,), True)
    arrive(2, 0)
    attend(0, (1, 5), False)
    arrive(2, 1)
    attend(1, (1, 5), False)
    arrive(3, 0)
    attend(0, (2, 6), False)
    arrive(3, 1)
    attend(1, (2, 6), False)
    attend(0, (3, 7), False)
    kv_wait(4, 0)
    attend(1, (3, 7), False)
    attend(0, (4,), False)
    kv_wait(4, 1)
    attend(1, (4,), False)

    for r in (2, 1, 3):
        at = pl.ds(r * 128, 128)
        ssend[r - 1] = ml[:, at]
        for m in range(4):
            osend[r - 1, m] = acc[m, :, at].astype(BF16)
        dev = (z, lax.rem(x + r, NX), y, c)
        send(osend.at[r - 1], orecv.at[r - 1], osd.at[r - 1], orv.at[r - 1], dev)
        send(ssend.at[r - 1], srecv.at[r - 1], ssd.at[r - 1], srv.at[r - 1], dev)

    wait(wp.at[0], loc.at[9])
    wait(wp.at[1], wrv.at[0])

    def turn(j, carry):
        for s in range(2):
            wpt[j, :, pl.ds(s * 256, 256)] = wp[s, j].T
        return carry

    lax.fori_loop(0, NY, turn, 0)

    for r in (1, 3, 2):
        wait(orecv.at[r - 1], orv.at[r - 1])
        wait(srecv.at[r - 1], srv.at[r - 1])
    for g in range(2):
        means = []
        for i in range(2):
            m = 2 * g + i
            tops = [ml[m : m + 1, 0:128]] + [srecv[r, m : m + 1, :] for r in range(3)]
            sums = [ml[4 + m : 5 + m, 0:128]] + [srecv[r, 4 + m : 5 + m, :] for r in range(3)]
            nums = [acc[m, :, 0:128]] + [orecv[r, m].astype(F32) for r in range(3)]
            top = functools.reduce(jnp.maximum, tops)
            w = [jnp.exp2((t - top) * SCALES[g]) for t in tops]
            total = functools.reduce(jnp.add, [a * b for a, b in zip(w, sums)])
            numer = functools.reduce(jnp.add, [a * b for a, b in zip(w, nums)])
            means.append(numer * ((1.0 if i == 0 else lam[g, 0]) / total))
        diff = means[0] - means[1]
        scale = lax.rsqrt(jnp.mean(diff * diff, axis=0, keepdims=True) + EPS)
        heads[0, pl.ds(g * 128, 128), :] = (diff * scale * cols[:, g : g + 1]).astype(BF16)
    send(heads.at[0], heads.at[1], hsd.at[0], hrv.at[0], partner)
    wait(heads.at[1], hrv.at[0])

    both = jnp.concatenate([heads[0], heads[1]], axis=0)
    for r in (4, 3, 5, 2, 6, 1, 7):
        t = lax.rem(y + r, NY)
        rsend[r - 1] = dot(wpt[t], both, 1, 0).astype(BF16)
        send(rsend.at[r - 1], rrecv.at[r - 1], rsd.at[r - 1], rrv.at[r - 1], (z, x, t, c))
    zt = ALPHA * tokt[...] + dot(wpt[y], both, 1, 0)
    for r in (1, 7, 2, 6, 3, 5, 4):
        wait(rrecv.at[r - 1], rrv.at[r - 1])
        zt = zt + rrecv[r - 1].astype(F32)

    sub8 = row_iota((8, 128))

    def local_stats(mean, dev2):
        return jnp.where(sub8 == 0, mean, jnp.where(sub8 == 1, dev2, 0.0))

    mean = jnp.mean(zt, axis=0, keepdims=True)
    dev2 = jnp.sum(jnp.square(zt - mean), axis=0, keepdims=True)
    stat1[0] = local_stats(mean, dev2)
    order = [(dy, dc) for dy in (4, 3, 5, 2, 6, 1, 7, 0) for dc in (1, 0) if dy or dc]
    for dy, dc in order:
        s = 2 * dy + dc
        send(
            stat1.at[0], stat1.at[s], s1s.at[s - 1], s1r.at[s - 1],
            (z, x, lax.rem(y + dy, NY), c if dc == 0 else other),
        )
    for s in range(1, 16):
        wait(stat1.at[s], s1r.at[s - 1])
    total = functools.reduce(jnp.add, [stat1[s] for s in range(16)])
    mean = total[0:1, :] * (1.0 / 16)
    spread = total[1:2, :] + 128.0 * functools.reduce(
        jnp.add, [jnp.square(stat1[s, 0:1, :] - mean) for s in range(16)]
    )
    scale = lax.rsqrt(spread * (1.0 / 2048) + EPS)
    normed = ((zt - mean) * scale * cols[:, 2:3]).astype(BF16)

    disp[...] = dot(dmat[...], normed, 1, 1).astype(BF16)

    def unit(j):
        return pl.ds(pl.multiple_of(j * CAP, CAP), CAP)

    arrive_at = unit(c * 16 + lax.rem(me, 16))

    def dispatch(j, carry):
        t = lax.rem(me + j, NSP)
        send(disp.at[unit(t)], xg.at[0, arrive_at], dps.at[0], dpr.at[0], (t // NX, lax.rem(t, NX), y, half))
        return carry

    lax.fori_loop(1, NSP, dispatch, 0)

    @pl.when(half == c)
    def _():
        xg[0, arrive_at, :] = disp[unit(me), :]

    @pl.when(half != c)
    def _():
        send(disp.at[unit(me)], xg.at[0, arrive_at], dps.at[0], dpr.at[0], partner)

    mixed[...] = normed.astype(F32).T * ALPHA
    for k, buf in enumerate((wg, wu, wd)):
        wait(buf.at[0], loc.at[10 + k])
        wait(buf.at[1], wrv.at[1 + k])

    def wait_units(ref, sem):
        @pl.when(half == c)
        def _():
            wait(ref.at[pl.ds(0, 496)], sem)

        @pl.when(half != c)
        def _():
            wait(ref, sem)

    wait_units(xg.at[0], dpr.at[0])

    pieces = (pl.ds(0, 256), pl.ds(256, 256))

    def xg_send(d, step, piece, src_slot, dst_slot):
        send(
            xg.at[src_slot, pieces[piece]], xg.at[dst_slot, pieces[piece]], xgs.at[d, step, piece],
            xgr.at[dst_slot, piece], (z, x, (yp, ym)[d], c),
        )

    def xg_wait(slot, piece):
        wait(xg.at[slot, pieces[piece]], xgr.at[slot, piece])

    def xg_arrive(d, piece):
        xg_wait(d, piece)
        if d < 3 or piece == 0:
            xg_send(0, d, piece, d, d + 1)
        xg_wait(4 + d, piece)
        if d < 3:
            xg_send(1, d, piece, 4 + d, 5 + d)
        elif piece == 1:
            xg_send(1, d, piece, 7, 4)

    def slot_y(slot):
        away = NY - slot if slot <= 4 else slot - 4
        return lax.rem(y + away, NY)

    def absorb(slot, piece, start=False):
        chunk = 2 * slot_y(slot) + piece
        at = pl.ds(pl.multiple_of(chunk * 128, 128), 128)
        rows_in = xg[slot, pieces[piece], :]
        for s in range(2):
            for w, a in ((wg, accg), (wu, accu)):
                value = dot(rows_in, w[s, at, :], 1, 0)
                a[s] = value if start else a[s] + value

    for piece in (0, 1):
        xg_send(0, 0, piece, 0, 1)
        xg_send(1, 0, piece, 0, 5)
    absorb(0, 0, True)
    absorb(0, 1)
    for d in (1, 2, 3):
        for piece in (0, 1):
            xg_arrive(d, piece)
            absorb(d, piece)
            absorb(4 + d, piece)
    for piece in (0, 1):
        xg_wait(4, piece)
        absorb(4, piece)
    for s in range(2):
        g = accg[s]
        act[s] = (g / (1.0 + jnp.exp(-g)) * accu[s]).astype(BF16)

    def produce(r):
        at = pl.ds(pl.multiple_of(lax.rem(y + r, NY) * 256, 256), 256)
        part[r] = dot(act[0], wd[0, :, at], 1, 0) + dot(act[1], wd[1, :, at], 1, 0)

    def away(d, h, step):
        return (4 - h - step) if d == 0 else (NY - 3 - h + step) % NY

    def length(d, h):
        return 4 - h if d == 0 else 3 + h

    def pass_on(d, h, step):
        value = part[away(d, h, step), :, h * 128 : h * 128 + 128]
        if step:
            wait(drecv.at[d, h, step - 1], ddr.at[d, h, step - 1])
            value = value + drecv[d, h, step - 1].astype(F32)
        dsend[d, h, step] = value.astype(BF16)
        send(
            dsend.at[d, h, step], drecv.at[d, h, step], dds.at[d, h, step], ddr.at[d, h, step],
            (z, x, (yp, ym)[d], c),
        )

    produce(4)
    pass_on(0, 0, 0)
    pass_on(1, 1, 0)
    produce(3)
    pass_on(0, 1, 0)
    produce(5)
    pass_on(1, 0, 0)
    for r in (2, 6, 1, 7, 0):
        produce(r)
    for step in (1, 2, 3):
        for h in (0, 1):
            for d in ((0, 1) if h == 0 else (1, 0)):
                if step < length(d, h):
                    pass_on(d, h, step)
    for h in (0, 1):
        value = part[0, :, h * 128 : h * 128 + 128]
        for d in range(2):
            last = length(d, h) - 1
            wait(drecv.at[d, h, last], ddr.at[d, h, last])
            value = value + drecv[d, h, last].astype(F32)
        eo[h] = value.astype(BF16)

    ret_at = unit(me)

    def give_back(i, carry):
        t = c * 16 + i
        for h in range(2):
            @pl.when(jnp.logical_or(t != me, c != h))
            def _():
                send(eo.at[h, unit(i)], ret.at[ret_at], rts.at[0], rtr.at[0], (t // NX, lax.rem(t, NX), y, h))
        return carry

    lax.fori_loop(0, 16, give_back, 0)

    @pl.when(half == c)
    def _():
        ret[ret_at, :] = eo[c, unit(lax.rem(me, 16)), :]

    wait_units(ret, rtr.at[0])

    zz = mixed[...]
    for k in range(2):
        zz = zz + gat[:, k : k + 1] * dot(pmat[k], ret[...], 1, 0)

    mean = jnp.mean(zz, axis=1, keepdims=True)
    dev = zz - mean
    dev2 = jnp.sum(dev * dev, axis=1, keepdims=True)
    fin[0] = dev.astype(BF16)
    packed = jnp.where(lane == 0, mean, jnp.where(lane == 1, dev2, 0.0)).T
    stat2[0] = packed[0:8, :]
    send(fin.at[0], fin.at[1], fns.at[0], fnr.at[0], partner)
    for dy, dc in order:
        s = 2 * dy + dc
        dev_id = (z, x, lax.rem(y + dy, NY), c if dc == 0 else other)
        send(stat2.at[0], stat2.at[s], s2s.at[s - 1], s2r.at[s - 1], dev_id)
    for dy in (4, 3, 5, 2, 6, 1, 7):
        send(fin.at[0], fin.at[2 * dy], fns.at[2 * dy - 1], fnr.at[2 * dy - 1], (z, x, lax.rem(y + dy, NY), c))
    for s in range(1, 16):
        wait(stat2.at[s], s2r.at[s - 1])
    total = functools.reduce(jnp.add, [stat2[s] for s in range(16)])
    mean = total[0:1, :] * (1.0 / 16)
    spread = total[1:2, :] + 128.0 * functools.reduce(
        jnp.add, [jnp.square(stat2[s, 0:1, :] - mean) for s in range(16)]
    )
    scale = lax.rsqrt(spread * (1.0 / 2048) + EPS)
    table = jnp.where(sub == 16, scale, 0.0)
    for s in range(16):
        table = jnp.where(sub == s, stat2[s, 0:1, :] - mean, table)
    table = table.T

    def finish(dy, dc):
        s = 2 * dy + dc
        j = 2 * lax.rem(y + NY - dy, NY) + (c if dc == 0 else other)
        value = (fin[s].astype(F32) + table[:, s : s + 1]) * table[:, 16:17] * g2[pl.ds(j, 1), :]
        outb[s] = value.astype(BF16)
        pltpu.make_async_copy(outb.at[s], out.at[:, col(j)], oud.at[s]).start()

    finish(0, 0)
    wait(fin.at[1], fnr.at[0])
    finish(0, 1)
    arrivals = (1, 7, 2, 6, 3, 5, 4)
    for i, dy in enumerate(arrivals):
        wait(fin.at[2 * dy], fnr.at[2 * dy - 1])
        send(fin.at[2 * dy], fin.at[2 * dy + 1], fns.at[2 * dy], fnr.at[2 * dy], partner)
        finish(dy, 0)
        if i:
            before_dy = arrivals[i - 1]
            wait(fin.at[2 * before_dy + 1], fnr.at[2 * before_dy])
            finish(before_dy, 1)
    wait(fin.at[9], fnr.at[8])
    finish(4, 1)

    for step in range(4):
        for piece in (0, 1):
            for d in range(2):
                if step < 3 or piece == d:
                    wait(kv.at[0, (N, B)[piece]], kvs.at[d, step, piece])
                    wait(xg.at[0, pieces[piece]], xgs.at[d, step, piece])
                if step < length(d, piece):
                    wait(dsend.at[d, piece, step], dds.at[d, piece, step])
    for r in range(3):
        wait(qraw.at[0], qsd.at[r])
        wait(osend.at[r], osd.at[r])
        wait(ssend.at[r], ssd.at[r])
    wait(wp.at[0], wsd.at[0])
    for k, buf in enumerate((wg, wu, wd)):
        wait(buf.at[0], wsd.at[1 + k])
    wait(heads.at[0], hsd.at[0])
    for r in range(7):
        wait(rsend.at[r], rsd.at[r])
    for s in range(15):
        wait(stat1.at[0], s1s.at[s])
        wait(stat2.at[0], s2s.at[s])
        wait(fin.at[0], fns.at[s])
    wait_units(disp, dps.at[0])
    wait_units(ret, rts.at[0])
    for s in range(16):
        wait(outb.at[s], oud.at[s])


def on_device(
    tokens, query_narrow, key_narrow, value_narrow, query_broad, key_broad, value_broad, mix_lambda,
    head_gain, proj_narrow, proj_broad, gain_one, gain_two, expert_ids, expert_gates,
    gate_weight, up_weight, down_weight,
):
    vmem, anywhere = pl.BlockSpec(memory_space=pltpu.VMEM), pl.BlockSpec(memory_space=pltpu.HBM)
    dma = pltpu.SemaphoreType.DMA
    bf = lambda *s: pltpu.VMEM(s, BF16)
    fl = lambda *s: pltpu.VMEM(s, F32)
    scratch = [
        bf(8, 5, 128, 128), bf(4, 3, 128, 128), bf(4, 512, 128), fl(4, 128, 512), fl(8, 512),
        bf(3, 4, 128, 128), bf(3, 4, 128, 128), fl(3, 8, 128), fl(3, 8, 128),
        bf(2, 8, 256, 128), bf(8, 128, 512), bf(128, 128), fl(128, 128),
        fl(8, 128), fl(128, 128), bf(512, 128), bf(2, 128, 512),
        bf(2, 256, 128), bf(7, 128, 128), bf(7, 128, 128), fl(16, 8, 128),
        fl(128, 128), bf(512, 128), bf(8, 512, 128),
        bf(2, 2048, 256), bf(2, 2048, 256), bf(2, 256, 2048),
        fl(2, 256, 256), fl(2, 256, 256), bf(2, 256, 256), fl(8, 256, 256),
        bf(2, 2, 4, 256, 128), bf(2, 2, 4, 256, 128),
        bf(512, 128), bf(2, 256, 128), bf(16, 128, 128), fl(16, 8, 128), bf(16, 128, 128),
        dma((13,)), dma((2, 4, 2)), dma((8, 2)), dma((3,)), dma((3,)), dma((4,)), dma((4,)),
        dma((3,)), dma((3,)), dma((3,)), dma((3,)), dma((1,)), dma((1,)), dma((7,)), dma((7,)),
        dma((15,)), dma((15,)), dma((1,)), dma((1,)), dma((2, 4, 2)), dma((8, 2)),
        dma((2, 2, 4)), dma((2, 2, 4)), dma((1,)), dma((1,)), dma((15,)), dma((15,)), dma((15,)), dma((15,)),
        dma((16,)),
    ]
    return pl.pallas_call(
        kernel,
        out_shape=jax.ShapeDtypeStruct((128, 2048), BF16),
        in_specs=[pl.BlockSpec(memory_space=pltpu.SMEM)] + [vmem] * 5 + [anywhere] * 12,
        out_specs=anywhere,
        scratch_shapes=scratch,
        compiler_params=pltpu.CompilerParams(
            collective_id=0, has_side_effects=True, vmem_limit_bytes=60 * 1024 * 1024
        ),
        name="layer",
    )(
        mix_lambda, expert_ids, expert_gates, head_gain, gain_one.reshape(16, 128), gain_two.reshape(16, 128),
        tokens, query_narrow, key_narrow, value_narrow, query_broad, key_broad, value_broad,
        proj_narrow, proj_broad, gate_weight, up_weight, down_weight,
    )


def solution(mesh):
    finer = Mesh(mesh.devices.reshape(NZ, NX, NY, 2), ("z", "x", "y", "c"))
    sp, tp = ("z", "x"), ("y", "c")
    return jax.shard_map(
        on_device,
        mesh=finer,
        in_specs=(
            P(sp, None), P(sp, tp), P(sp, tp), P(sp, tp), P(sp, tp), P(sp, tp), P(sp, tp), P(None, tp),
            P(), P(tp, None), P(tp, None), P(), P(), P(sp, None), P(sp, None),
            P(sp, None, tp), P(sp, None, tp), P(sp, tp, None),
        ),
        out_specs=P(sp, None),
        check_vma=False,
    )
```

time: 380 us -> 129 us (0.34); the launches traced: 376 us -> 129 us
  waiting for transfers between devices: 155 us -> 0 us
  blocking collectives: 133 us -> 0 us
  Pallas kernels: 0 us -> 124 us
  local copies, waits for them, and re-layouts: 30.6 us -> 4.69 us
  other arithmetic: 16.5 us -> 0 us
  starting transfers between devices: 13.7 us -> 0 us
  between operations: 13.7 us -> 0.01 us
  matrix products: 12.8 us -> 0 us
    all_to_all x3 -> x0, blocking collectives: 131 us -> none  [the longest x1 59.9 us: on_device(): lax.all_to_all(outgoing, 'sp', split_axis=1, concat_axis=1, tiled=True)]
    pallas_call x0 -> x1, Pallas kernels: none -> 124 us  [on_device(): pl.pallas_call(kernel, out_shape=jax.ShapeDtypeStruct((128, 2048), BF16),...]
    all_gather x2 -> x0, waiting for transfers between devices: 123 us -> none  [the longest x1 92.7 us: in_one_piece(): lax.all_gather(both, axis, axis=dim, tiled=True)]
    all_to_all x2 -> x0, waiting for transfers between devices: 32.3 us -> none  [the longest x1 17.2 us: sum_at_owner(): pieces = lax.all_to_all(cut_along(value, dim, size), axis, 0, 0, tiled=True)]
    all_to_all x2 -> x0, starting transfers between devices: 13.7 us -> none  [the longest x1 10.2 us: sum_at_owner(): pieces = lax.all_to_all(cut_along(value, dim, size), axis, 0, 0, tiled=True)]
    dot_general x8 -> x0, matrix products: 12.8 us -> none  [the longest x1 5.51 us: on_device(): jnp.einsum('rxf,xfd->rxd', activated, down_weight, preferred_element_type...]
    reduce_sum x12 -> x0, other arithmetic: 11.8 us -> none  [the longest x1 4.74 us: on_device(): jnp.sum(expert_gates[:, :, None] * picked.astype(jnp.float32), axis=1)]
    scatter x1 -> x0, local copies, waits for them, and re-layouts: 4.43 us -> none  [on_device(): jnp.zeros((CAP * experts_all, model_width), jnp.bfloat16).at[position]]
  transfers between devices with their start and end apart: 4 -> 0, of which waited for: 4 -> 0; matrix products, arithmetic and copies ran while one was open for 1% -> 0% of each run, Pallas kernels for 0% -> 0%
where the time goes in v1:
time: 129 us
  Pallas kernels  124 us (96%)
  local copies, waits for them, and re-layouts  4.69 us (4%)
    pallas_call x1, Pallas kernels, on_device(): pl.pallas_call(kernel, out_shape=jax.ShapeDtypeStruct((128, 2048), BF16),...  124 us
    unnamed x10, local copies, waits for them, and re-layouts  4.69 us

profile of v1, /device:TPU:1, one launch (start us, length us, event | category | flops | bytes accessed | tf_op | source)
XLA Modules:
  0.0 129.0 jit_solution(14507019343296525008)
XLA Ops:
  0.0 0.0 copy-start.2
  0.0 0.7 copy-done.2
  0.7 0.0 copy-start
  0.7 0.7 copy.19.lam
  1.3 0.0 copy-done
  1.3 0.0 copy-start.1
  1.3 0.7 copy.20.ids
  2.1 0.0 copy-done.1
  2.1 0.7 copy.21.gates
  2.8 124.3 %layer.1 = bf16[128,2048]{1,0:T(8,128)(2,1)} custom-call(f32[2,1]{1,0:T(2,128)} %copy.19.lam, s32[128,2]{1,0:T(8,128)} %copy.20.ids, f32[128,2]{1,0:T(8,128)} %copy.21.gates, f32[2,128]{1,0:T(2,128)} %hgain.1, f32[16,128]{1,0:T(8,128)} %bitcast.2, f32[16,128]{1,0:T(8,128)} %bitcast.3, bf16[128,2048]{1,0:T(8,128)(2,1)} %tok.1, bf16[128,128]{1,0:T(8,128)(2,1)} %qn.1, ...), custom_call_target="tpu_custom_call" | custom-call | tf_op jit(solution)/shard_map/layer/pallas_call | solution.py:553
  127.1 1.9 %copy.23 = bf16[128,2048]{1,0:T(8,128)(2,1)} copy(bf16[128,2048]{1,0:T(8,128)(2,1)} %layer.1) | data formatting | bytes 1048576
Async XLA Ops:
  0.0 0.7 copy-start.2
  0.7 0.7 copy-start
  1.3 0.7 copy-start.1

commit v2 on v1

v2 whole, which is shorter than its diff:
```python
import functools

import jax
import jax.numpy as jnp
from jax import lax
from jax.experimental import pallas as pl
from jax.experimental.pallas import tpu as pltpu
from jax.sharding import Mesh
from jax.sharding import PartitionSpec as P

MESH = pl.DeviceIdType.MESH
NZ, NX, NY = 8, 4, 8
NSP = NZ * NX
CAP = 16
F32, BF16 = jnp.float32, jnp.bfloat16
ALPHA = 8.0**0.25
EPS = 1e-05
LOG2E = 1.4426950408889634
SCALES = (64**-0.5 * LOG2E, 128**-0.5 * LOG2E)


def dot(a, b, ca, cb):
    return lax.dot_general(a, b, (((ca,), (cb,)), ((), ())), preferred_element_type=F32)


def wait(ref, sem):
    pltpu.make_async_copy(ref, ref, sem).wait()


def send(src, dst, send_sem, recv_sem, dev):
    pltpu.make_async_remote_copy(
        src_ref=src, dst_ref=dst, send_sem=send_sem, recv_sem=recv_sem, device_id=dev, device_id_type=MESH
    ).start()


def row_iota(shape):
    return lax.broadcasted_iota(jnp.int32, shape, 0)


def lane_iota(shape):
    return lax.broadcasted_iota(jnp.int32, shape, 1)


def kernel(
    lam_in, ids_in, gates_in, hgain_in, g1_in, g2_in, tok, qn, kn, vn, qb, kb, vb, pn, pb, gw, uw, dw,
    out,
    kv, qraw, qs, acc, ml, osend, orecv, ssend, srecv, wp, wpt, tokraw, tokt, cols, dmat, pmat, gat,
    heads, rsend, rrecv, stat1, mixed, disp, xg, wg, wu, wd, accg, accu, act, part, dsend, drecv,
    ret, eo, fin, stat2, lam, ids, gates, hgain, g1, g2, outb,
    loc, kvs, kvr, qsd, qrv, wsd, wrv, osd, orv, ssd, srv, hsd, hrv, rsd, rrv, s1s, s1r, dps, dpr,
    xgs, xgr, dds, ddr, rts, rtr, fns, fnr, s2s, s2r, smalls, ysem, oud,
):
    z, x, y, c = (lax.axis_index(n) for n in ("z", "x", "y", "c"))
    me = z * NX + x
    own = 2 * y + c
    other = 1 - c
    half = me // 16
    zp, zm = lax.rem(z + 1, NZ), lax.rem(z + NZ - 1, NZ)
    yp, ym = lax.rem(y + 1, NY), lax.rem(y + NY - 1, NY)
    partner = (z, x, y, other)

    def col(j):
        return pl.ds(pl.multiple_of(j * 128, 128), 128)

    def local(i, src, dst):
        cp = pltpu.make_async_copy(src, dst, loc.at[i])
        cp.start()
        return cp

    first = [
        local(0, kn, kv.at[0, 0]), local(1, vn, kv.at[0, 1]),
        local(2, kb.at[:, pl.ds(0, 128)], kv.at[0, 2]), local(3, kb.at[:, pl.ds(128, 128)], kv.at[0, 3]),
        local(4, vb, kv.at[0, 4]),
        local(5, qn, qraw.at[0, 0]), local(6, qb.at[:, pl.ds(0, 128)], qraw.at[0, 1]),
        local(7, qb.at[:, pl.ds(128, 128)], qraw.at[0, 2]),
    ]
    tokcp = local(8, tok.at[:, col(own)], tokraw)
    small = []
    for i, (src, dst) in enumerate(
        ((ids_in, ids), (gates_in, gates), (hgain_in, hgain), (g1_in, g1), (g2_in, g2), (lam_in, lam))
    ):
        small.append(pltpu.make_async_copy(src, dst, smalls.at[i]))
        small[-1].start()

    barrier = pltpu.get_barrier_semaphore()
    sides_y = ((z, x, yp, c), (z, x, ym, c))
    for dev in [(zp, x, y, c), (zm, x, y, c), partner, *sides_y] + [
        (z, lax.rem(x + r, NX), y, c) for r in range(1, NX)
    ]:
        pl.semaphore_signal(barrier, inc=1, device_id=dev, device_id_type=MESH)
    pl.semaphore_wait(barrier, 8)

    def relay(k):
        for dev in sides_y:
            pl.semaphore_signal(ysem.at[k], inc=1, device_id=dev, device_id_type=MESH)

    def relayed(k):
        pl.semaphore_wait(ysem.at[k], 2)

    for cp in first:
        cp.wait()
    def kv_send(d, step, piece, src_slot, dst_slot):
        send(
            kv.at[src_slot, piece], kv.at[dst_slot, piece], kvs.at[d, step, piece], kvr.at[dst_slot, piece],
            ((zp, zm)[d], x, y, c),
        )

    def kv_wait(slot, piece):
        wait(kv.at[slot, piece], kvr.at[slot, piece])

    for piece in range(5):
        kv_send(0, 0, piece, 0, 1)
        kv_send(1, 0, piece, 0, 5)
    q_parts = (pl.ds(0, 1), pl.ds(1, 2))
    for k in range(2):
        for r in (2, 1, 3):
            send(
                qraw.at[0, q_parts[k]], qraw.at[r, q_parts[k]], qsd.at[r - 1, k], qrv.at[r - 1, k],
                (z, lax.rem(x + NX - r, NX), y, c),
            )
    relay(0)

    def proj(j, carry):
        for k, w in enumerate((pn, pb)):
            dst = pl.ds(k * 128, 128)
            pltpu.make_async_copy(w.at[:, col(2 * j + c)], wp.at[0, j, dst], loc.at[9]).start()
            send(w.at[:, col(2 * j + other)], wp.at[1, j, dst], wsd.at[0], wrv.at[0], partner)
        return carry

    for k, (w, buf) in enumerate(((gw, wg), (uw, wu), (dw, wd))):
        local(10 + k, w.at[0], buf.at[0])

    def swap_expert():
        for k, (w, buf) in enumerate(((gw, wg), (uw, wu), (dw, wd))):
            send(w.at[0], buf.at[1], wsd.at[1 + k], wrv.at[1 + k], partner)

    lane = lane_iota((128, 128))
    sub = row_iota((128, 128))
    for cp in small:
        cp.wait()
    idr = ids[...].astype(F32)
    rows_e = row_iota((NSP, 128)).astype(F32)
    hot = [(idr[k : k + 1, :] == rows_e).astype(F32) for k in range(2)]
    upper = (sub < lane).astype(F32).astype(BF16)
    before = dot((hot[0] + hot[1]).astype(BF16), upper, 1, 0)
    pos = [
        idr[k : k + 1, :] * float(CAP) + jnp.sum(before * hot[k], axis=0, keepdims=True) for k in range(2)
    ]
    rows_s = row_iota((CAP * NSP, 128)).astype(F32)
    dmat[...] = ((pos[0] == rows_s).astype(F32) + (pos[1] == rows_s).astype(F32)).astype(BF16)
    posc = jnp.where(
        sub == 0, pos[0],
        jnp.where(sub == 1, pos[1], jnp.where(sub == 2, gates[0:1, :], jnp.where(sub == 3, gates[1:2, :], 0.0))),
    ).T
    gat[...] = posc
    lanes_s = lane_iota((128, CAP * NSP)).astype(F32)
    for k in range(2):
        pmat[k] = (posc[:, k : k + 1] == lanes_s).astype(F32).astype(BF16)
    gain_rows = jnp.where(
        sub == 0, hgain[0:1, :], jnp.where(sub == 1, hgain[1:2, :], jnp.where(sub == 2, g1[pl.ds(own, 1), :], 0.0))
    )
    cols[...] = gain_rows.T
    tokcp.wait()
    tokt[...] = tokraw[...].astype(F32).T

    low = lane < 64

    def queries(k):
        for r in (1, 3, 2):
            wait(qraw.at[r, q_parts[k]], qrv.at[r - 1, k])
        for r in range(NX):
            at = pl.ds(r * 128, 128)
            if k == 0:
                narrow = qraw[r, 0]
                qs[0, at, :] = jnp.where(low, narrow, jnp.zeros_like(narrow))
                qs[1, at, :] = jnp.where(low, jnp.zeros_like(narrow), narrow)
            else:
                qs[2, at, :] = qraw[r, 1]
                qs[3, at, :] = qraw[r, 2]

    def attend(group, slots, start=False):
        for m in (2 * group, 2 * group + 1):
            k_at = 0 if group == 0 else m
            v_at = 1 if group == 0 else 4
            query = qs[m]
            scores = [dot(kv[s, k_at], query, 1, 1) for s in slots]
            top = functools.reduce(jnp.maximum, [jnp.max(s, axis=0, keepdims=True) for s in scores])
            if not start:
                old = ml[m : m + 1, :]
                top = jnp.maximum(old, top)
            expo = [jnp.exp2((s - top) * SCALES[group]) for s in scores]
            total = functools.reduce(jnp.add, [jnp.sum(e, axis=0, keepdims=True) for e in expo])
            numer = functools.reduce(
                jnp.add, [dot(kv[s, v_at], e.astype(BF16), 0, 0) for s, e in zip(slots, expo)]
            )
            if start:
                acc[m] = numer
                ml[4 + m : 5 + m, :] = total
            else:
                shrink = jnp.exp2((old - top) * SCALES[group])
                acc[m] = acc[m] * shrink + numer
                ml[4 + m : 5 + m, :] = ml[4 + m : 5 + m, :] * shrink + total
            ml[m : m + 1, :] = top

    def arrive(d, group):
        for piece in ((0, 1), (2, 3, 4))[group]:
            kv_wait(d, piece)
            if d < 3 or group == 0:
                kv_send(0, d, piece, d, d + 1)
            kv_wait(4 + d, piece)
            if d < 3:
                kv_send(1, d, piece, 4 + d, 5 + d)
            elif group == 1:
                kv_send(1, d, piece, 7, 4)

    def far(group):
        for piece in ((0, 1), (2, 3, 4))[group]:
            kv_wait(4, piece)

    def share(group):
        for r in (2, 1, 3):
            at = pl.ds(r * 128, 128)
            for i in range(2):
                osend[r - 1, 2 * group + i] = acc[2 * group + i, :, at].astype(BF16)
            dev = (z, lax.rem(x + r, NX), y, c)
            pair = pl.ds(2 * group, 2)
            send(
                osend.at[r - 1, pair], orecv.at[r - 1, pair], osd.at[r - 1, group], orv.at[r - 1, group], dev
            )
            if group == 1:
                ssend[r - 1] = ml[:, at]
                send(ssend.at[r - 1], srecv.at[r - 1], ssd.at[r - 1], srv.at[r - 1], dev)

    arrive(1, 0)
    relayed(0)
    relay(1)
    queries(0)
    arrive(1, 1)
    attend(0, (0,), True)
    arrive(2, 0)
    attend(0, (1, 5))
    relayed(1)
    relay(2)
    queries(1)
    arrive(2, 1)
    lax.fori_loop(0, NY, proj, 0)
    attend(1, (0,), True)
    arrive(3, 0)
    attend(1, (1, 5))
    relayed(2)
    arrive(3, 1)
    swap_expert()
    attend(0, (2, 6))
    attend(1, (2, 6))
    attend(0, (3, 7))
    far(0)
    attend(0, (4,))
    share(0)
    attend(1, (3, 7))
    far(1)
    attend(1, (4,))
    share(1)

    wait(wp.at[0], loc.at[9])
    wait(wp.at[1], wrv.at[0])

    def turn(j, carry):
        for s in range(2):
            wpt[j, :, pl.ds(s * 256, 256)] = wp[s, j].T
        return carry

    lax.fori_loop(0, NY, turn, 0)

    for r in (1, 3, 2):
        for k in range(2):
            wait(orecv.at[r - 1, pl.ds(2 * k, 2)], orv.at[r - 1, k])
        wait(srecv.at[r - 1], srv.at[r - 1])
    for g in range(2):
        means = []
        for i in range(2):
            m = 2 * g + i
            tops = [ml[m : m + 1, 0:128]] + [srecv[r, m : m + 1, :] for r in range(3)]
            sums = [ml[4 + m : 5 + m, 0:128]] + [srecv[r, 4 + m : 5 + m, :] for r in range(3)]
            nums = [acc[m, :, 0:128]] + [orecv[r, m].astype(F32) for r in range(3)]
            top = functools.reduce(jnp.maximum, tops)
            w = [jnp.exp2((t - top) * SCALES[g]) for t in tops]
            total = functools.reduce(jnp.add, [a * b for a, b in zip(w, sums)])
            numer = functools.reduce(jnp.add, [a * b for a, b in zip(w, nums)])
            means.append(numer * ((1.0 if i == 0 else lam[0:1, g : g + 1]) / total))
        diff = means[0] - means[1]
        scale = lax.rsqrt(jnp.mean(diff * diff, axis=0, keepdims=True) + EPS)
        heads[0, pl.ds(g * 128, 128), :] = (diff * scale * cols[:, g : g + 1]).astype(BF16)
    send(heads.at[0], heads.at[1], hsd.at[0], hrv.at[0], partner)
    wait(heads.at[1], hrv.at[0])

    both = jnp.concatenate([heads[0], heads[1]], axis=0)
    for r in (4, 3, 5, 2, 6, 1, 7):
        t = lax.rem(y + r, NY)
        rsend[r - 1] = dot(wpt[t], both, 1, 0).astype(BF16)
        send(rsend.at[r - 1], rrecv.at[r - 1], rsd.at[r - 1], rrv.at[r - 1], (z, x, t, c))
    zt = ALPHA * tokt[...] + dot(wpt[y], both, 1, 0)
    for r in (1, 7, 2, 6, 3, 5, 4):
        wait(rrecv.at[r - 1], rrv.at[r - 1])
        zt = zt + rrecv[r - 1].astype(F32)

    sub8 = row_iota((8, 128))

    def local_stats(mean, dev2):
        return jnp.where(sub8 == 0, mean, jnp.where(sub8 == 1, dev2, 0.0))

    mean = jnp.mean(zt, axis=0, keepdims=True)
    dev2 = jnp.sum(jnp.square(zt - mean), axis=0, keepdims=True)
    stat1[0] = local_stats(mean, dev2)
    order = [(dy, dc) for dy in (4, 3, 5, 2, 6, 1, 7, 0) for dc in (1, 0) if dy or dc]
    for dy, dc in order:
        s = 2 * dy + dc
        send(
            stat1.at[0], stat1.at[s], s1s.at[s - 1], s1r.at[s - 1],
            (z, x, lax.rem(y + dy, NY), c if dc == 0 else other),
        )
    for s in range(1, 16):
        wait(stat1.at[s], s1r.at[s - 1])
    total = functools.reduce(jnp.add, [stat1[s] for s in range(16)])
    mean = total[0:1, :] * (1.0 / 16)
    spread = total[1:2, :] + 128.0 * functools.reduce(
        jnp.add, [jnp.square(stat1[s, 0:1, :] - mean) for s in range(16)]
    )
    scale = lax.rsqrt(spread * (1.0 / 2048) + EPS)
    normed = ((zt - mean) * scale * cols[:, 2:3]).astype(BF16)

    disp[...] = dot(dmat[...], normed, 1, 1).astype(BF16)

    def unit(j):
        return pl.ds(pl.multiple_of(j * CAP, CAP), CAP)

    arrive_at = unit(c * 16 + lax.rem(me, 16))

    def dispatch(j, carry):
        t = lax.rem(me + j, NSP)
        send(disp.at[unit(t)], xg.at[0, arrive_at], dps.at[0], dpr.at[0], (t // NX, lax.rem(t, NX), y, half))
        return carry

    lax.fori_loop(1, NSP, dispatch, 0)

    @pl.when(half == c)
    def _():
        xg[0, arrive_at, :] = disp[unit(me), :]

    @pl.when(half != c)
    def _():
        send(disp.at[unit(me)], xg.at[0, arrive_at], dps.at[0], dpr.at[0], partner)

    mixed[...] = normed.astype(F32).T * ALPHA
    for k, buf in enumerate((wg, wu, wd)):
        wait(buf.at[0], loc.at[10 + k])
        wait(buf.at[1], wrv.at[1 + k])

    def wait_units(ref, sem):
        @pl.when(half == c)
        def _():
            wait(ref.at[pl.ds(0, 496)], sem)

        @pl.when(half != c)
        def _():
            wait(ref, sem)

    wait_units(xg.at[0], dpr.at[0])

    def piece_of(h, k):
        return pl.ds(k * 256 + h * 128, 128)

    def xg_send(d, step, h, k, src_slot, dst_slot):
        send(
            xg.at[src_slot, piece_of(h, k)], xg.at[dst_slot, piece_of(h, k)], xgs.at[d, step, 2 * h + k],
            xgr.at[dst_slot, 2 * h + k], (z, x, (yp, ym)[d], c),
        )

    def xg_wait(slot, h, k):
        wait(xg.at[slot, piece_of(h, k)], xgr.at[slot, 2 * h + k])

    def xg_arrive(d, h, k):
        xg_wait(d, h, k)
        if d < 3 or k == 0:
            xg_send(0, d, h, k, d, d + 1)
        xg_wait(4 + d, h, k)
        if d < 3:
            xg_send(1, d, h, k, 4 + d, 5 + d)
        elif k == 1:
            xg_send(1, d, h, k, 7, 4)

    def slot_y(slot):
        away = NY - slot if slot <= 4 else slot - 4
        return lax.rem(y + away, NY)

    def absorb(slot, h, start=False):
        at = pl.ds(pl.multiple_of(slot_y(slot) * 256, 256), 256)
        rows_in = jnp.concatenate([xg[slot, piece_of(h, 0), :], xg[slot, piece_of(h, 1), :]], axis=1)
        for s in range(2):
            for w, a in ((wg, accg), (wu, accu)):
                value = dot(rows_in, w[s, at, :], 1, 0)
                a[h, s] = value if start else a[h, s] + value

    for h in (0, 1):
        for k in (0, 1):
            xg_send(0, 0, h, k, 0, 1)
            xg_send(1, 0, h, k, 0, 5)
    for h in (0, 1):
        absorb(0, h, True)
    for d in (1, 2, 3):
        for h in (0, 1):
            for k in (0, 1):
                xg_arrive(d, h, k)
            absorb(d, h)
            absorb(4 + d, h)

    def produce(h, r):
        at = pl.ds(pl.multiple_of(lax.rem(y + r, NY) * 256, 256), 256)
        part[h, r] = dot(act[h, 0], wd[0, :, at], 1, 0) + dot(act[h, 1], wd[1, :, at], 1, 0)

    def away(d, k, step):
        return (4 - k - step) if d == 0 else (NY - 3 - k + step) % NY

    def length(d, k):
        return 4 - k if d == 0 else 3 + k

    def pass_on(d, h, k, step):
        value = part[h, away(d, k, step), :, k * 128 : k * 128 + 128]
        p = 2 * h + k
        if step:
            wait(drecv.at[d, p, step - 1], ddr.at[d, p, step - 1])
            value = value + drecv[d, p, step - 1].astype(F32)
        dsend[d, p, step] = value.astype(BF16)
        send(
            dsend.at[d, p, step], drecv.at[d, p, step], dds.at[d, p, step], ddr.at[d, p, step],
            (z, x, (yp, ym)[d], c),
        )

    for h in (0, 1):
        for k in (0, 1):
            xg_wait(4, h, k)
        absorb(4, h)
        for s in range(2):
            g = accg[h, s]
            act[h, s] = (g / (1.0 + jnp.exp(-g)) * accu[h, s]).astype(BF16)
        produce(h, 4)
        pass_on(0, h, 0, 0)
        pass_on(1, h, 1, 0)
        produce(h, 3)
        pass_on(0, h, 1, 0)
        produce(h, 5)
        pass_on(1, h, 0, 0)
        for r in (2, 6, 1, 7, 0):
            produce(h, r)
    for step in (1, 2, 3):
        for h in (0, 1):
            for d, k in ((0, 0), (1, 1), (0, 1), (1, 0)):
                if step < length(d, k):
                    pass_on(d, h, k, step)

    ret_at = unit(me)

    def give_back(i, carry):
        t = c * 16 + i
        for k in range(2):
            @pl.when(jnp.logical_or(t != me, c != k))
            def _():
                send(eo.at[k, unit(i)], ret.at[ret_at], rts.at[0], rtr.at[0], (t // NX, lax.rem(t, NX), y, k))
        return carry

    for h in (0, 1):
        for k in (0, 1):
            value = part[h, 0, :, k * 128 : k * 128 + 128]
            for d in range(2):
                last, p = length(d, k) - 1, 2 * h + k
                wait(drecv.at[d, p, last], ddr.at[d, p, last])
                value = value + drecv[d, p, last].astype(F32)
            eo[k, pl.ds(h * 128, 128), :] = value.astype(BF16)
        lax.fori_loop(8 * h, 8 * h + 8, give_back, 0)

    @pl.when(half == c)
    def _():
        ret[ret_at, :] = eo[c, unit(lax.rem(me, 16)), :]

    wait_units(ret, rtr.at[0])

    zz = mixed[...]
    for k in range(2):
        zz = zz + gat[:, 2 + k : 3 + k] * dot(pmat[k], ret[...], 1, 0)

    mean = jnp.mean(zz, axis=1, keepdims=True)
    dev = zz - mean
    dev2 = jnp.sum(dev * dev, axis=1, keepdims=True)
    fin[0] = dev.astype(BF16)
    packed = jnp.where(lane == 0, mean, jnp.where(lane == 1, dev2, 0.0)).T
    stat2[0] = packed[0:8, :]
    send(fin.at[0], fin.at[1], fns.at[0], fnr.at[0], partner)
    for dy, dc in order:
        s = 2 * dy + dc
        dev_id = (z, x, lax.rem(y + dy, NY), c if dc == 0 else other)
        send(stat2.at[0], stat2.at[s], s2s.at[s - 1], s2r.at[s - 1], dev_id)
    for dy in (4, 3, 5, 2, 6, 1, 7):
        send(fin.at[0], fin.at[2 * dy], fns.at[2 * dy - 1], fnr.at[2 * dy - 1], (z, x, lax.rem(y + dy, NY), c))
    for s in range(1, 16):
        wait(stat2.at[s], s2r.at[s - 1])
    total = functools.reduce(jnp.add, [stat2[s] for s in range(16)])
    mean = total[0:1, :] * (1.0 / 16)
    spread = total[1:2, :] + 128.0 * functools.reduce(
        jnp.add, [jnp.square(stat2[s, 0:1, :] - mean) for s in range(16)]
    )
    scale = lax.rsqrt(spread * (1.0 / 2048) + EPS)
    table = jnp.where(sub == 16, scale, 0.0)
    for s in range(16):
        table = jnp.where(sub == s, stat2[s, 0:1, :] - mean, table)
    table = table.T

    def finish(dy, dc):
        s = 2 * dy + dc
        j = 2 * lax.rem(y + NY - dy, NY) + (c if dc == 0 else other)
        value = (fin[s].astype(F32) + table[:, s : s + 1]) * table[:, 16:17] * g2[pl.ds(j, 1), :]
        outb[s] = value.astype(BF16)
        pltpu.make_async_copy(outb.at[s], out.at[:, col(j)], oud.at[s]).start()

    finish(0, 0)
    wait(fin.at[1], fnr.at[0])
    finish(0, 1)
    arrivals = (1, 7, 2, 6, 3, 5, 4)
    for i, dy in enumerate(arrivals):
        wait(fin.at[2 * dy], fnr.at[2 * dy - 1])
        send(fin.at[2 * dy], fin.at[2 * dy + 1], fns.at[2 * dy], fnr.at[2 * dy], partner)
        finish(dy, 0)
        if i:
            before_dy = arrivals[i - 1]
            wait(fin.at[2 * before_dy + 1], fnr.at[2 * before_dy])
            finish(before_dy, 1)
    wait(fin.at[9], fnr.at[8])
    finish(4, 1)

    for step in range(4):
        for d in range(2):
            for piece in range(5):
                if step < 3 or (piece >= 2) == d:
                    wait(kv.at[0, piece], kvs.at[d, step, piece])
            for p in range(4):
                if step < 3 or p % 2 == d:
                    wait(xg.at[0, pl.ds(0, 128)], xgs.at[d, step, p])
                if step < length(d, p % 2):
                    wait(dsend.at[d, p, step], dds.at[d, p, step])
    for r in range(3):
        for k in range(2):
            wait(qraw.at[0, q_parts[k]], qsd.at[r, k])
            wait(osend.at[r, pl.ds(2 * k, 2)], osd.at[r, k])
        wait(ssend.at[r], ssd.at[r])
    wait(wp.at[0], wsd.at[0])
    for k, buf in enumerate((wg, wu, wd)):
        wait(buf.at[0], wsd.at[1 + k])
    wait(heads.at[0], hsd.at[0])
    for r in range(7):
        wait(rsend.at[r], rsd.at[r])
    for s in range(15):
        wait(stat1.at[0], s1s.at[s])
        wait(stat2.at[0], s2s.at[s])
        wait(fin.at[0], fns.at[s])
    wait_units(disp, dps.at[0])
    wait_units(ret, rts.at[0])
    for s in range(16):
        wait(outb.at[s], oud.at[s])


def on_device(
    tokens, query_narrow, key_narrow, value_narrow, query_broad, key_broad, value_broad, mix_lambda,
    head_gain, proj_narrow, proj_broad, gain_one, gain_two, expert_ids, expert_gates,
    gate_weight, up_weight, down_weight,
):
    memory = pl.BlockSpec(memory_space=pltpu.HBM)
    dma = pltpu.SemaphoreType.DMA
    bf = lambda *s: pltpu.VMEM(s, BF16)
    fl = lambda *s: pltpu.VMEM(s, F32)
    scratch = [
        bf(8, 5, 128, 128), bf(4, 3, 128, 128), bf(4, 512, 128), fl(4, 128, 512), fl(8, 512),
        bf(3, 4, 128, 128), bf(3, 4, 128, 128), fl(3, 8, 128), fl(3, 8, 128),
        bf(2, 8, 256, 128), bf(8, 128, 512), bf(128, 128), fl(128, 128),
        fl(128, 128), bf(512, 128), bf(2, 128, 512), fl(128, 128),
        bf(2, 256, 128), bf(7, 128, 128), bf(7, 128, 128), fl(16, 8, 128),
        fl(128, 128), bf(512, 128), bf(8, 512, 128),
        bf(2, 2048, 256), bf(2, 2048, 256), bf(2, 256, 2048),
        fl(2, 2, 128, 256), fl(2, 2, 128, 256), bf(2, 2, 128, 256), fl(2, 8, 128, 256),
        bf(2, 4, 4, 128, 128), bf(2, 4, 4, 128, 128),
        bf(512, 128), bf(2, 256, 128), bf(16, 128, 128), fl(16, 8, 128),
        fl(1, 2), pltpu.VMEM((2, 128), jnp.int32), fl(2, 128), fl(2, 128), fl(16, 128), fl(16, 128),
        bf(16, 128, 128),
        dma((13,)), dma((2, 4, 5)), dma((8, 5)), dma((3, 2)), dma((3, 2)), dma((4,)), dma((4,)),
        dma((3, 2)), dma((3, 2)), dma((3,)), dma((3,)), dma((1,)), dma((1,)), dma((7,)), dma((7,)),
        dma((15,)), dma((15,)), dma((1,)), dma((1,)), dma((2, 4, 4)), dma((8, 4)),
        dma((2, 4, 4)), dma((2, 4, 4)), dma((1,)), dma((1,)), dma((15,)), dma((15,)), dma((15,)), dma((15,)),
        dma((6,)), pltpu.SemaphoreType.REGULAR((3,)), dma((16,)),
    ]
    return pl.pallas_call(
        kernel,
        out_shape=jax.ShapeDtypeStruct((128, 2048), BF16),
        in_specs=[memory] * 18,
        out_specs=memory,
        scratch_shapes=scratch,
        compiler_params=pltpu.CompilerParams(
            collective_id=0, has_side_effects=True, vmem_limit_bytes=60 * 1024 * 1024
        ),
        name="layer",
    )(
        mix_lambda.T, expert_ids.T, expert_gates.T, head_gain, gain_one.reshape(16, 128), gain_two.reshape(16, 128),
        tokens, query_narrow, key_narrow, value_narrow, query_broad, key_broad, value_broad,
        proj_narrow, proj_broad, gate_weight, up_weight, down_weight,
    )


def solution(mesh):
    finer = Mesh(mesh.devices.reshape(NZ, NX, NY, 2), ("z", "x", "y", "c"))
    sp, tp = ("z", "x"), ("y", "c")
    return jax.shard_map(
        on_device,
        mesh=finer,
        in_specs=(
            P(sp, None), P(sp, tp), P(sp, tp), P(sp, tp), P(sp, tp), P(sp, tp), P(sp, tp), P(None, tp),
            P(), P(tp, None), P(tp, None), P(), P(), P(sp, None), P(sp, None),
            P(sp, None, tp), P(sp, None, tp), P(sp, tp, None),
        ),
        out_specs=P(sp, None),
        check_vma=False,
    )
```

time: 129 us -> 113 us (0.88)
  Pallas kernels: 124 us -> 111 us
  local copies, waits for them, and re-layouts: 4.69 us -> 1.88 us
    pallas_call x1, Pallas kernels: 124 us -> 111 us  [on_device(): pl.pallas_call(kernel, out_shape=jax.ShapeDtypeStruct((128, 2048), BF16),...]
    unnamed x10 -> x1, local copies, waits for them, and re-layouts: 4.69 us -> 1.88 us
where the time goes in v2:
time: 113 us
  Pallas kernels  111 us (98%)
  local copies, waits for them, and re-layouts  1.88 us (2%)
    pallas_call x1, Pallas kernels, on_device(): pl.pallas_call(kernel, out_shape=jax.ShapeDtypeStruct((128, 2048), BF16),...  111 us

profile of v2, /device:TPU:1, one launch (start us, length us, event | category | flops | bytes accessed | tf_op | source)
XLA Modules:
  0.0 113.2 jit_solution(13436624461335314443)
XLA Ops:
  0.0 111.3 %layer.1 = bf16[128,2048]{1,0:T(8,128)(2,1)} custom-call(f32[1,2]{1,0:T(1,128)} %bitcast.9, s32[2,128]{1,0:T(2,128)} %bitcast.7, f32[2,128]{1,0:T(2,128)} %bitcast.8, f32[2,128]{1,0:T(2,128)} %hgain_in.1, f32[16,128]{1,0:T(8,128)} %bitcast.5, f32[16,128]{1,0:T(8,128)} %bitcast.6, bf16[128,2048]{1,0:T(8,128)(2,1)} %tok.1, bf16[128,128]{1,0:T(8,128)(2,1)} %qn.1, ...), custom_call_target="tpu_custom_call" | custom-call | tf_op jit(solution)/shard_map/layer/pallas_call | solution.py:597
  111.4 1.9 %copy.20 = bf16[128,2048]{1,0:T(8,128)(2,1)} copy(bf16[128,2048]{1,0:T(8,128)(2,1)} %layer.1) | data formatting | bytes 1048576

commit v3 on v2

--- a/solution.py
+++ b/solution.py
@@ -46,9 +46,9 @@
     out,
     kv, qraw, qs, acc, ml, osend, orecv, ssend, srecv, wp, wpt, tokraw, tokt, cols, dmat, pmat, gat,
     heads, rsend, rrecv, stat1, mixed, disp, xg, wg, wu, wd, accg, accu, act, part, dsend, drecv,
-    ret, eo, fin, stat2, lam, ids, gates, hgain, g1, g2, outb,
+    ret, eo, fin, stat2, lam, ids, gates, hgain, g1, g2, outb, blocks, gsum, tdisp, sx,
     loc, kvs, kvr, qsd, qrv, wsd, wrv, osd, orv, ssd, srv, hsd, hrv, rsd, rrv, s1s, s1r, dps, dpr,
-    xgs, xgr, dds, ddr, rts, rtr, fns, fnr, s2s, s2r, smalls, ysem, oud,
+    xgs, xgr, dds, ddr, rts, rtr, fns, fnr, s2s, s2r, smalls, ysem, oud, tds, tdr,
 ):
     z, x, y, c = (lax.axis_index(n) for n in ("z", "x", "y", "c"))
     me = z * NX + x
@@ -179,28 +179,28 @@
                 qs[3, at, :] = qraw[r, 2]
 
     def attend(group, slots, start=False):
+        v_at = 1 if group == 0 else 4
+        turned = [kv[s, v_at].T for s in slots]
         for m in (2 * group, 2 * group + 1):
             k_at = 0 if group == 0 else m
-            v_at = 1 if group == 0 else 4
-            query = qs[m]
-            scores = [dot(kv[s, k_at], query, 1, 1) for s in slots]
-            top = functools.reduce(jnp.maximum, [jnp.max(s, axis=0, keepdims=True) for s in scores])
-            if not start:
-                old = ml[m : m + 1, :]
-                top = jnp.maximum(old, top)
-            expo = [jnp.exp2((s - top) * SCALES[group]) for s in scores]
-            total = functools.reduce(jnp.add, [jnp.sum(e, axis=0, keepdims=True) for e in expo])
-            numer = functools.reduce(
-                jnp.add, [dot(kv[s, v_at], e.astype(BF16), 0, 0) for s, e in zip(slots, expo)]
-            )
-            if start:
-                acc[m] = numer
-                ml[4 + m : 5 + m, :] = total
-            else:
-                shrink = jnp.exp2((old - top) * SCALES[group])
-                acc[m] = acc[m] * shrink + numer
-                ml[4 + m : 5 + m, :] = ml[4 + m : 5 + m, :] * shrink + total
-            ml[m : m + 1, :] = top
+            for at in [pl.ds(0, 512)] if len(slots) == 2 else [pl.ds(0, 256), pl.ds(256, 256)]:
+                query = qs[m, at, :]
+                scores = [dot(kv[s, k_at], query, 1, 1) for s in slots]
+                top = functools.reduce(jnp.maximum, [jnp.max(s, axis=0, keepdims=True) for s in scores])
+                if not start:
+                    old = ml[m : m + 1, at]
+                    top = jnp.maximum(old, top)
+                expo = [jnp.exp2((s - top) * SCALES[group]) for s in scores]
+                total = functools.reduce(jnp.add, [jnp.sum(e, axis=0, keepdims=True) for e in expo])
+                numer = functools.reduce(jnp.add, [dot(v, e.astype(BF16), 1, 0) for v, e in zip(turned, expo)])
+                if start:
+                    acc[m, :, at] = numer
+                    ml[4 + m : 5 + m, at] = total
+                else:
+                    shrink = jnp.exp2((old - top) * SCALES[group])
+                    acc[m, :, at] = acc[m, :, at] * shrink + numer
+                    ml[4 + m : 5 + m, at] = ml[4 + m : 5 + m, at] * shrink + total
+                ml[m : m + 1, at] = top
 
     def arrive(d, group):
         for piece in ((0, 1), (2, 3, 4))[group]:
@@ -299,6 +299,23 @@
         rsend[r - 1] = dot(wpt[t], both, 1, 0).astype(BF16)
         send(rsend.at[r - 1], rrecv.at[r - 1], rsd.at[r - 1], rrv.at[r - 1], (z, x, t, c))
     zt = ALPHA * tokt[...] + dot(wpt[y], both, 1, 0)
+
+    for k, buf in enumerate((wg, wu, wd)):
+        wait(buf.at[0], loc.at[10 + k])
+        wait(buf.at[1], wrv.at[1 + k])
+    sub32 = row_iota((32, 128))
+    for s in range(16):
+        dy, dc = s // 2, s % 2
+        j = 2 * lax.rem(y + NY - dy, NY) + (c if dc == 0 else other)
+        gain = g1[pl.ds(j, 1), :]
+        top = gain.astype(BF16).astype(F32)
+        blocks[:, col(j)] = jnp.where(sub32 == s, top, jnp.where(sub32 == 16 + s, gain - top, 0.0)).astype(BF16)
+    for k, w in enumerate((wg, wu)):
+        for s in range(2):
+            value = dot(blocks[...], w[s], 1, 0)
+            value = value[0:16] + value[16:32]
+            top = value.astype(BF16).astype(F32)
+            gsum[k, s] = jnp.concatenate([top, top, value - top, jnp.zeros((80, 256), F32)], axis=0).astype(BF16)
     for r in (1, 7, 2, 6, 3, 5, 4):
         wait(rrecv.at[r - 1], rrv.at[r - 1])
         zt = zt + rrecv[r - 1].astype(F32)
@@ -318,6 +335,29 @@
             stat1.at[0], stat1.at[s], s1s.at[s - 1], s1r.at[s - 1],
             (z, x, lax.rem(y + dy, NY), c if dc == 0 else other),
         )
+    raised = ((zt - mean) * cols[:, 2:3]).astype(BF16)
+    disp[...] = dot(dmat[...], raised, 1, 1).astype(BF16)
+
+    def unit(j):
+        return pl.ds(pl.multiple_of(j * CAP, CAP), CAP)
+
+    arrive_at = unit(c * 16 + lax.rem(me, 16))
+
+    def dispatch(j, carry):
+        t = lax.rem(me + j, NSP)
+        send(disp.at[unit(t)], xg.at[0, arrive_at], dps.at[0], dpr.at[0], (t // NX, lax.rem(t, NX), y, half))
+        return carry
+
+    lax.fori_loop(1, NSP, dispatch, 0)
+
+    @pl.when(half == c)
+    def _():
+        xg[0, arrive_at, :] = disp[unit(me), :]
+
+    @pl.when(half != c)
+    def _():
+        send(disp.at[unit(me)], xg.at[0, arrive_at], dps.at[0], dpr.at[0], partner)
+
     for s in range(1, 16):
         wait(stat1.at[s], s1r.at[s - 1])
     total = functools.reduce(jnp.add, [stat1[s] for s in range(16)])
@@ -326,34 +366,32 @@
         jnp.add, [jnp.square(stat1[s, 0:1, :] - mean) for s in range(16)]
     )
     scale = lax.rsqrt(spread * (1.0 / 2048) + EPS)
-    normed = ((zt - mean) * scale * cols[:, 2:3]).astype(BF16)
-
-    disp[...] = dot(dmat[...], normed, 1, 1).astype(BF16)
-
-    def unit(j):
-        return pl.ds(pl.multiple_of(j * CAP, CAP), CAP)
-
-    arrive_at = unit(c * 16 + lax.rem(me, 16))
-
-    def dispatch(j, carry):
+    sub16 = row_iota((16, 128))
+    shift = jnp.zeros((16, 128), F32)
+    for s in range(16):
+        shift = jnp.where(sub16 == s, stat1[s, 0:1, :] - mean, shift)
+    top = shift.astype(BF16).astype(F32)
+    one = scale.astype(BF16).astype(F32)
+    two = (scale - one).astype(BF16).astype(F32)
+    parts = jnp.where(
+        sub16 == 0, one, jnp.where(sub16 == 1, two, jnp.where(sub16 == 2, scale - one - two, 0.0))
+    )
+    table = jnp.concatenate([top, shift - top, top, parts, jnp.zeros((64, 128), F32)], axis=0).astype(BF16)
+    tdisp[...] = dot(dmat[...], table, 1, 1).astype(BF16)
+
+    def follow(j, carry):
         t = lax.rem(me + j, NSP)
-        send(disp.at[unit(t)], xg.at[0, arrive_at], dps.at[0], dpr.at[0], (t // NX, lax.rem(t, NX), y, half))
+        send(
+            tdisp.at[unit(t)], sx.at[unit(lax.rem(me, 16))], tds.at[0], tdr.at[0], (t // NX, lax.rem(t, NX), y, c)
+        )
         return carry
-
-    lax.fori_loop(1, NSP, dispatch, 0)
 
     @pl.when(half == c)
     def _():
-        xg[0, arrive_at, :] = disp[unit(me), :]
-
-    @pl.when(half != c)
-    def _():
-        send(disp.at[unit(me)], xg.at[0, arrive_at], dps.at[0], dpr.at[0], partner)
-
-    mixed[...] = normed.astype(F32).T * ALPHA
-    for k, buf in enumerate((wg, wu, wd)):
-        wait(buf.at[0], loc.at[10 + k])
-        wait(buf.at[1], wrv.at[1 + k])
+        lax.fori_loop(1, NSP, follow, 0)
+        sx[unit(lax.rem(me, 16)), :] = tdisp[unit(me), :]
+
+    mixed[...] = ((zt - mean) * scale * cols[:, 2:3]).astype(BF16).astype(F32).T * ALPHA
 
     def wait_units(ref, sem):
         @pl.when(half == c)
@@ -435,13 +473,25 @@
             (z, x, (yp, ym)[d], c),
         )
 
+    @pl.when(half == c)
+    def _():
+        wait(sx.at[pl.ds(0, 240)], tdr.at[0])
+
+    @pl.when(half != c)
+    def _():
+        wait(sx, tdr.at[0])
+
     for h in (0, 1):
+        stat = sx[h * 128 : h * 128 + 128, :]
+        scales = stat[:, 48:64].astype(F32)
+        scales = scales[:, 0:1] + scales[:, 1:2] + scales[:, 2:3]
+        shifts = [[dot(stat, gsum[k, s], 1, 0) for s in range(2)] for k in range(2)]
         for k in (0, 1):
             xg_wait(4, h, k)
         absorb(4, h)
         for s in range(2):
-            g = accg[h, s]
-            act[h, s] = (g / (1.0 + jnp.exp(-g)) * accu[h, s]).astype(BF16)
+            g = (accg[h, s] + shifts[0][s]) * scales
+            act[h, s] = (g / (1.0 + jnp.exp(-g)) * ((accu[h, s] + shifts[1][s]) * scales)).astype(BF16)
         produce(h, 4)
         pass_on(0, h, 0, 0)
         pass_on(1, h, 1, 0)
@@ -561,6 +611,11 @@
         wait(stat2.at[0], s2s.at[s])
         wait(fin.at[0], fns.at[s])
     wait_units(disp, dps.at[0])
+
+    @pl.when(half == c)
+    def _():
+        wait(tdisp.at[pl.ds(0, 496)], tds.at[0])
+
     wait_units(ret, rts.at[0])
     for s in range(16):
         wait(outb.at[s], oud.at[s])
@@ -587,12 +642,12 @@
         bf(2, 4, 4, 128, 128), bf(2, 4, 4, 128, 128),
         bf(512, 128), bf(2, 256, 128), bf(16, 128, 128), fl(16, 8, 128),
         fl(1, 2), pltpu.VMEM((2, 128), jnp.int32), fl(2, 128), fl(2, 128), fl(16, 128), fl(16, 128),
-        bf(16, 128, 128),
+        bf(16, 128, 128), bf(32, 2048), bf(2, 2, 128, 256), bf(512, 128), bf(256, 128),
         dma((13,)), dma((2, 4, 5)), dma((8, 5)), dma((3, 2)), dma((3, 2)), dma((4,)), dma((4,)),
         dma((3, 2)), dma((3, 2)), dma((3,)), dma((3,)), dma((1,)), dma((1,)), dma((7,)), dma((7,)),
         dma((15,)), dma((15,)), dma((1,)), dma((1,)), dma((2, 4, 4)), dma((8, 4)),
         dma((2, 4, 4)), dma((2, 4, 4)), dma((1,)), dma((1,)), dma((15,)), dma((15,)), dma((15,)), dma((15,)),
-        dma((6,)), pltpu.SemaphoreType.REGULAR((3,)), dma((16,)),
+        dma((6,)), pltpu.SemaphoreType.REGULAR((3,)), dma((16,)), dma((1,)), dma((1,)),
     ]
     return pl.pallas_call(
         kernel,

time: 113 us -> 108 us (0.956)
  Pallas kernels: 111 us -> 106 us
    pallas_call x1, Pallas kernels: 111 us -> 106 us  [on_device(): pl.pallas_call(kernel, out_shape=jax.ShapeDtypeStruct((128, 2048), BF16),...]
where the time goes in v3:
time: 108 us
  Pallas kernels  106 us (98%)
  local copies, waits for them, and re-layouts  1.88 us (2%)
    pallas_call x1, Pallas kernels, on_device(): pl.pallas_call(kernel, out_shape=jax.ShapeDtypeStruct((128, 2048), BF16),...  106 us

profile of v3, /device:TPU:1, one launch (start us, length us, event | category | flops | bytes accessed | tf_op | source)
XLA Modules:
  0.0 107.9 jit_solution(557370398148486498)
XLA Ops:
  0.0 106.0 %layer.1 = bf16[128,2048]{1,0:T(8,128)(2,1)} custom-call(f32[1,2]{1,0:T(1,128)} %bitcast.9, s32[2,128]{1,0:T(2,128)} %bitcast.7, f32[2,128]{1,0:T(2,128)} %bitcast.8, f32[2,128]{1,0:T(2,128)} %hgain_in.1, f32[16,128]{1,0:T(8,128)} %bitcast.5, f32[16,128]{1,0:T(8,128)} %bitcast.6, bf16[128,2048]{1,0:T(8,128)(2,1)} %tok.1, bf16[128,128]{1,0:T(8,128)(2,1)} %qn.1, ...), custom_call_target="tpu_custom_call" | custom-call | tf_op jit(solution)/shard_map/layer/pallas_call | solution.py:652
  106.0 1.9 %copy.20 = bf16[128,2048]{1,0:T(8,128)(2,1)} copy(bf16[128,2048]{1,0:T(8,128)(2,1)} %layer.1) | data formatting | bytes 1048576

commit v4 on v3

--- a/solution.py
+++ b/solution.py
@@ -179,28 +179,29 @@
                 qs[3, at, :] = qraw[r, 2]
 
     def attend(group, slots, start=False):
-        v_at = 1 if group == 0 else 4
-        turned = [kv[s, v_at].T for s in slots]
-        for m in (2 * group, 2 * group + 1):
-            k_at = 0 if group == 0 else m
-            for at in [pl.ds(0, 512)] if len(slots) == 2 else [pl.ds(0, 256), pl.ds(256, 256)]:
-                query = qs[m, at, :]
-                scores = [dot(kv[s, k_at], query, 1, 1) for s in slots]
-                top = functools.reduce(jnp.maximum, [jnp.max(s, axis=0, keepdims=True) for s in scores])
-                if not start:
-                    old = ml[m : m + 1, at]
-                    top = jnp.maximum(old, top)
-                expo = [jnp.exp2((s - top) * SCALES[group]) for s in scores]
-                total = functools.reduce(jnp.add, [jnp.sum(e, axis=0, keepdims=True) for e in expo])
-                numer = functools.reduce(jnp.add, [dot(v, e.astype(BF16), 1, 0) for v, e in zip(turned, expo)])
-                if start:
-                    acc[m, :, at] = numer
-                    ml[4 + m : 5 + m, at] = total
-                else:
-                    shrink = jnp.exp2((old - top) * SCALES[group])
-                    acc[m, :, at] = acc[m, :, at] * shrink + numer
-                    ml[4 + m : 5 + m, at] = ml[4 + m : 5 + m, at] * shrink + total
-                ml[m : m + 1, at] = top
+        turned = [kv[s, 1 if group == 0 else 4].T for s in slots]
+        tiles = [(m, pl.ds(q * 256, 256)) for m in (2 * group, 2 * group + 1) for q in range(2)]
+        scores = [[dot(kv[s, 0 if group == 0 else m], qs[m, at, :], 1, 1) for s in slots] for m, at in tiles]
+        state = []
+        for (m, at), score in zip(tiles, scores):
+            top = functools.reduce(jnp.maximum, [jnp.max(s, axis=0, keepdims=True) for s in score])
+            old = None
+            if not start:
+                old = ml[m : m + 1, at]
+                top = jnp.maximum(old, top)
+            expo = [jnp.exp2((s - top) * SCALES[group]) for s in score]
+            total = functools.reduce(jnp.add, [jnp.sum(e, axis=0, keepdims=True) for e in expo])
+            state.append((old, top, total, [e.astype(BF16) for e in expo]))
+        for (m, at), (old, top, total, expo) in zip(tiles, state):
+            numer = functools.reduce(jnp.add, [dot(v, e, 1, 0) for v, e in zip(turned, expo)])
+            if start:
+                acc[m, :, at] = numer
+                ml[4 + m : 5 + m, at] = total
+            else:
+                shrink = jnp.exp2((old - top) * SCALES[group])
+                acc[m, :, at] = acc[m, :, at] * shrink + numer
+                ml[4 + m : 5 + m, at] = ml[4 + m : 5 + m, at] * shrink + total
+            ml[m : m + 1, at] = top
 
     def arrive(d, group):
         for piece in ((0, 1), (2, 3, 4))[group]:
@@ -291,14 +292,16 @@
         scale = lax.rsqrt(jnp.mean(diff * diff, axis=0, keepdims=True) + EPS)
         heads[0, pl.ds(g * 128, 128), :] = (diff * scale * cols[:, g : g + 1]).astype(BF16)
     send(heads.at[0], heads.at[1], hsd.at[0], hrv.at[0], partner)
+    for r in (4, 3, 5, 2, 6, 1, 7, 0):
+        part[0, r, :, 0:128] = dot(wpt[lax.rem(y + r, NY), :, 0:256], heads[0], 1, 0)
     wait(heads.at[1], hrv.at[0])
 
-    both = jnp.concatenate([heads[0], heads[1]], axis=0)
-    for r in (4, 3, 5, 2, 6, 1, 7):
+    far_first = (4, 3, 5, 2, 6, 1, 7)
+    for r in far_first:
         t = lax.rem(y + r, NY)
-        rsend[r - 1] = dot(wpt[t], both, 1, 0).astype(BF16)
+        rsend[r - 1] = (part[0, r, :, 0:128] + dot(wpt[t, :, 256:512], heads[1], 1, 0)).astype(BF16)
         send(rsend.at[r - 1], rrecv.at[r - 1], rsd.at[r - 1], rrv.at[r - 1], (z, x, t, c))
-    zt = ALPHA * tokt[...] + dot(wpt[y], both, 1, 0)
+    zt = ALPHA * tokt[...] + part[0, 0, :, 0:128] + dot(wpt[y, :, 256:512], heads[1], 1, 0)
 
     for k, buf in enumerate((wg, wu, wd)):
         wait(buf.at[0], loc.at[10 + k])
@@ -316,14 +319,14 @@
             value = value[0:16] + value[16:32]
             top = value.astype(BF16).astype(F32)
             gsum[k, s] = jnp.concatenate([top, top, value - top, jnp.zeros((80, 256), F32)], axis=0).astype(BF16)
-    for r in (1, 7, 2, 6, 3, 5, 4):
+    for r in far_first:
         wait(rrecv.at[r - 1], rrv.at[r - 1])
         zt = zt + rrecv[r - 1].astype(F32)
 
-    sub8 = row_iota((8, 128))
+    sub2 = row_iota((2, 128))
 
     def local_stats(mean, dev2):
-        return jnp.where(sub8 == 0, mean, jnp.where(sub8 == 1, dev2, 0.0))
+        return jnp.where(sub2 == 0, mean, dev2)
 
     mean = jnp.mean(zt, axis=0, keepdims=True)
     dev2 = jnp.sum(jnp.square(zt - mean), axis=0, keepdims=True)
@@ -542,49 +545,14 @@
     dev2 = jnp.sum(dev * dev, axis=1, keepdims=True)
     fin[0] = dev.astype(BF16)
     packed = jnp.where(lane == 0, mean, jnp.where(lane == 1, dev2, 0.0)).T
-    stat2[0] = packed[0:8, :]
+    stat2[0] = packed[0:2, :]
     send(fin.at[0], fin.at[1], fns.at[0], fnr.at[0], partner)
     for dy, dc in order:
         s = 2 * dy + dc
         dev_id = (z, x, lax.rem(y + dy, NY), c if dc == 0 else other)
         send(stat2.at[0], stat2.at[s], s2s.at[s - 1], s2r.at[s - 1], dev_id)
-    for dy in (4, 3, 5, 2, 6, 1, 7):
+    for dy in far_first:
         send(fin.at[0], fin.at[2 * dy], fns.at[2 * dy - 1], fnr.at[2 * dy - 1], (z, x, lax.rem(y + dy, NY), c))
-    for s in range(1, 16):
-        wait(stat2.at[s], s2r.at[s - 1])
-    total = functools.reduce(jnp.add, [stat2[s] for s in range(16)])
-    mean = total[0:1, :] * (1.0 / 16)
-    spread = total[1:2, :] + 128.0 * functools.reduce(
-        jnp.add, [jnp.square(stat2[s, 0:1, :] - mean) for s in range(16)]
-    )
-    scale = lax.rsqrt(spread * (1.0 / 2048) + EPS)
-    table = jnp.where(sub == 16, scale, 0.0)
-    for s in range(16):
-        table = jnp.where(sub == s, stat2[s, 0:1, :] - mean, table)
-    table = table.T
-
-    def finish(dy, dc):
-        s = 2 * dy + dc
-        j = 2 * lax.rem(y + NY - dy, NY) + (c if dc == 0 else other)
-        value = (fin[s].astype(F32) + table[:, s : s + 1]) * table[:, 16:17] * g2[pl.ds(j, 1), :]
-        outb[s] = value.astype(BF16)
-        pltpu.make_async_copy(outb.at[s], out.at[:, col(j)], oud.at[s]).start()
-
-    finish(0, 0)
-    wait(fin.at[1], fnr.at[0])
-    finish(0, 1)
-    arrivals = (1, 7, 2, 6, 3, 5, 4)
-    for i, dy in enumerate(arrivals):
-        wait(fin.at[2 * dy], fnr.at[2 * dy - 1])
-        send(fin.at[2 * dy], fin.at[2 * dy + 1], fns.at[2 * dy], fnr.at[2 * dy], partner)
-        finish(dy, 0)
-        if i:
-            before_dy = arrivals[i - 1]
-            wait(fin.at[2 * before_dy + 1], fnr.at[2 * before_dy])
-            finish(before_dy, 1)
-    wait(fin.at[9], fnr.at[8])
-    finish(4, 1)
-
     for step in range(4):
         for d in range(2):
             for piece in range(5):
@@ -608,8 +576,6 @@
         wait(rsend.at[r], rsd.at[r])
     for s in range(15):
         wait(stat1.at[0], s1s.at[s])
-        wait(stat2.at[0], s2s.at[s])
-        wait(fin.at[0], fns.at[s])
     wait_units(disp, dps.at[0])
 
     @pl.when(half == c)
@@ -617,6 +583,44 @@
         wait(tdisp.at[pl.ds(0, 496)], tds.at[0])
 
     wait_units(ret, rts.at[0])
+    for s in range(1, 16):
+        wait(stat2.at[s], s2r.at[s - 1])
+    total = functools.reduce(jnp.add, [stat2[s] for s in range(16)])
+    mean = total[0:1, :] * (1.0 / 16)
+    spread = total[1:2, :] + 128.0 * functools.reduce(
+        jnp.add, [jnp.square(stat2[s, 0:1, :] - mean) for s in range(16)]
+    )
+    scale = lax.rsqrt(spread * (1.0 / 2048) + EPS)
+    table = jnp.where(sub == 16, scale, 0.0)
+    for s in range(16):
+        table = jnp.where(sub == s, stat2[s, 0:1, :] - mean, table)
+    table = table.T
+
+    def finish(dy, dc):
+        s = 2 * dy + dc
+        j = 2 * lax.rem(y + NY - dy, NY) + (c if dc == 0 else other)
+        value = (fin[s].astype(F32) + table[:, s : s + 1]) * table[:, 16:17] * g2[pl.ds(j, 1), :]
+        outb[s] = value.astype(BF16)
+        pltpu.make_async_copy(outb.at[s], out.at[:, col(j)], oud.at[s]).start()
+
+    finish(0, 0)
+    wait(fin.at[1], fnr.at[0])
+    finish(0, 1)
+    arrivals = far_first
+    for i, dy in enumerate(arrivals):
+        wait(fin.at[2 * dy], fnr.at[2 * dy - 1])
+        send(fin.at[2 * dy], fin.at[2 * dy + 1], fns.at[2 * dy], fnr.at[2 * dy], partner)
+        finish(dy, 0)
+        if i:
+            before_dy = arrivals[i - 1]
+            wait(fin.at[2 * before_dy + 1], fnr.at[2 * before_dy])
+            finish(before_dy, 1)
+    wait(fin.at[15], fnr.at[14])
+    finish(7, 1)
+
+    for s in range(15):
+        wait(stat2.at[0], s2s.at[s])
+        wait(fin.at[0], fns.at[s])
     for s in range(16):
         wait(outb.at[s], oud.at[s])
 
@@ -635,12 +639,12 @@
         bf(3, 4, 128, 128), bf(3, 4, 128, 128), fl(3, 8, 128), fl(3, 8, 128),
         bf(2, 8, 256, 128), bf(8, 128, 512), bf(128, 128), fl(128, 128),
         fl(128, 128), bf(512, 128), bf(2, 128, 512), fl(128, 128),
-        bf(2, 256, 128), bf(7, 128, 128), bf(7, 128, 128), fl(16, 8, 128),
+        bf(2, 256, 128), bf(7, 128, 128), bf(7, 128, 128), fl(16, 2, 128),
         fl(128, 128), bf(512, 128), bf(8, 512, 128),
         bf(2, 2048, 256), bf(2, 2048, 256), bf(2, 256, 2048),
         fl(2, 2, 128, 256), fl(2, 2, 128, 256), bf(2, 2, 128, 256), fl(2, 8, 128, 256),
         bf(2, 4, 4, 128, 128), bf(2, 4, 4, 128, 128),
-        bf(512, 128), bf(2, 256, 128), bf(16, 128, 128), fl(16, 8, 128),
+        bf(512, 128), bf(2, 256, 128), bf(16, 128, 128), fl(16, 2, 128),
         fl(1, 2), pltpu.VMEM((2, 128), jnp.int32), fl(2, 128), fl(2, 128), fl(16, 128), fl(16, 128),
         bf(16, 128, 128), bf(32, 2048), bf(2, 2, 128, 256), bf(512, 128), bf(256, 128),
         dma((13,)), dma((2, 4, 5)), dma((8, 5)), dma((3, 2)), dma((3, 2)), dma((4,)), dma((4,)),

time: 108 us -> 105 us (0.972)
  Pallas kernels: 106 us -> 103 us
    pallas_call x1, Pallas kernels: 106 us -> 103 us  [on_device(): pl.pallas_call(kernel, out_shape=jax.ShapeDtypeStruct((128, 2048), BF16),...]
where the time goes in v4:
time: 105 us
  Pallas kernels  103 us (98%)
  local copies, waits for them, and re-layouts  1.88 us (2%)
    pallas_call x1, Pallas kernels, on_device(): pl.pallas_call(kernel, out_shape=jax.ShapeDtypeStruct((128, 2048), BF16),...  103 us

profile of v4, /device:TPU:1, one launch (start us, length us, event | category | flops | bytes accessed | tf_op | source)
XLA Modules:
  0.0 105.2 jit_solution(2520192761915558601)
XLA Ops:
  0.0 103.3 %layer.1 = bf16[128,2048]{1,0:T(8,128)(2,1)} custom-call(f32[1,2]{1,0:T(1,128)} %bitcast.9, s32[2,128]{1,0:T(2,128)} %bitcast.7, f32[2,128]{1,0:T(2,128)} %bitcast.8, f32[2,128]{1,0:T(2,128)} %hgain_in.1, f32[16,128]{1,0:T(8,128)} %bitcast.5, f32[16,128]{1,0:T(8,128)} %bitcast.6, bf16[128,2048]{1,0:T(8,128)(2,1)} %tok.1, bf16[128,128]{1,0:T(8,128)(2,1)} %qn.1, ...), custom_call_target="tpu_custom_call" | custom-call | tf_op jit(solution)/shard_map/layer/pallas_call | solution.py:656
  103.4 1.9 %copy.20 = bf16[128,2048]{1,0:T(8,128)(2,1)} copy(bf16[128,2048]{1,0:T(8,128)(2,1)} %layer.1) | data formatting | bytes 1048576

commit v5 on v4

--- a/solution.py
+++ b/solution.py
@@ -54,7 +54,9 @@
     me = z * NX + x
     own = 2 * y + c
     other = 1 - c
-    half = me // 16
+    half = lax.rem(x, 2)
+    place = (x // 2) * NZ + z
+    far_z, far_x = (4, 3, 5, 2, 6, 1, 7, 0), (2, 1, 3, 0)
     zp, zm = lax.rem(z + 1, NZ), lax.rem(z + NZ - 1, NZ)
     yp, ym = lax.rem(y + 1, NY), lax.rem(y + NY - 1, NY)
     partner = (z, x, y, other)
@@ -296,12 +298,24 @@
         part[0, r, :, 0:128] = dot(wpt[lax.rem(y + r, NY), :, 0:256], heads[0], 1, 0)
     wait(heads.at[1], hrv.at[0])
 
-    far_first = (4, 3, 5, 2, 6, 1, 7)
-    for r in far_first:
-        t = lax.rem(y + r, NY)
-        rsend[r - 1] = (part[0, r, :, 0:128] + dot(wpt[t, :, 256:512], heads[1], 1, 0)).astype(BF16)
-        send(rsend.at[r - 1], rrecv.at[r - 1], rsd.at[r - 1], rrv.at[r - 1], (z, x, t, c))
-    zt = ALPHA * tokt[...] + part[0, 0, :, 0:128] + dot(wpt[y, :, 256:512], heads[1], 1, 0)
+    def product(r):
+        return part[0, r, :, 0:128] + dot(wpt[lax.rem(y + r, NY), :, 256:512], heads[1], 1, 0)
+
+    def give(r):
+        send(rsend.at[r - 1], rrecv.at[r - 1], rsd.at[r - 1], rrv.at[r - 1], (z, x, lax.rem(y + r, NY), c))
+
+    ends = (pl.ds(0, 64), pl.ds(64, 64))
+    rsend[3] = product(4).astype(BF16)
+    for k, r in enumerate((3, 5)):
+        send(
+            rsend.at[3, ends[k]], rrecv.at[3, ends[k]], rsd.at[(3, 7)[k]], rrv.at[(3, 7)[k]],
+            (z, x, lax.rem(y + r, NY), c),
+        )
+    for r in (3, 5, 2, 6):
+        rsend[r - 1] = product(r).astype(BF16)
+        give(r)
+    near = [product(1), product(7)]
+    zt = ALPHA * tokt[...] + product(0)
 
     for k, buf in enumerate((wg, wu, wd)):
         wait(buf.at[0], loc.at[10 + k])
@@ -319,7 +333,15 @@
             value = value[0:16] + value[16:32]
             top = value.astype(BF16).astype(F32)
             gsum[k, s] = jnp.concatenate([top, top, value - top, jnp.zeros((80, 256), F32)], axis=0).astype(BF16)
-    for r in far_first:
+    for k, r in enumerate((1, 7)):
+        wait(rrecv.at[3, ends[k]], rrv.at[(3, 7)[k]])
+        passed = rrecv[3, ends[k], :].astype(F32)
+        rest = near[k][64:128] if k == 0 else near[k][0:64]
+        mine = near[k][0:64] if k == 0 else near[k][64:128]
+        rsend[r - 1, ends[k], :] = (mine + passed).astype(BF16)
+        rsend[r - 1, ends[1 - k], :] = rest.astype(BF16)
+        give(r)
+    for r in (3, 5, 2, 6, 1, 7):
         wait(rrecv.at[r - 1], rrv.at[r - 1])
         zt = zt + rrecv[r - 1].astype(F32)
 
@@ -344,14 +366,13 @@
     def unit(j):
         return pl.ds(pl.multiple_of(j * CAP, CAP), CAP)
 
-    arrive_at = unit(c * 16 + lax.rem(me, 16))
-
-    def dispatch(j, carry):
-        t = lax.rem(me + j, NSP)
-        send(disp.at[unit(t)], xg.at[0, arrive_at], dps.at[0], dpr.at[0], (t // NX, lax.rem(t, NX), y, half))
-        return carry
-
-    lax.fori_loop(1, NSP, dispatch, 0)
+    arrive_at = unit(c * 16 + place)
+
+    for dz in far_z:
+        for dx in far_x:
+            if dz or dx:
+                tz, tx = lax.rem(z + dz, NZ), lax.rem(x + dx, NX)
+                send(disp.at[unit(tz * NX + tx)], xg.at[0, arrive_at], dps.at[0], dpr.at[0], (tz, tx, y, half))
 
     @pl.when(half == c)
     def _():
@@ -382,17 +403,14 @@
     table = jnp.concatenate([top, shift - top, top, parts, jnp.zeros((64, 128), F32)], axis=0).astype(BF16)
     tdisp[...] = dot(dmat[...], table, 1, 1).astype(BF16)
 
-    def follow(j, carry):
-        t = lax.rem(me + j, NSP)
-        send(
-            tdisp.at[unit(t)], sx.at[unit(lax.rem(me, 16))], tds.at[0], tdr.at[0], (t // NX, lax.rem(t, NX), y, c)
-        )
-        return carry
-
     @pl.when(half == c)
     def _():
-        lax.fori_loop(1, NSP, follow, 0)
-        sx[unit(lax.rem(me, 16)), :] = tdisp[unit(me), :]
+        for dz in far_z:
+            for dx in far_x:
+                if dz or dx:
+                    tz, tx = lax.rem(z + dz, NZ), lax.rem(x + dx, NX)
+                    send(tdisp.at[unit(tz * NX + tx)], sx.at[unit(place)], tds.at[0], tdr.at[0], (tz, tx, y, c))
+        sx[unit(place), :] = tdisp[unit(me), :]
 
     mixed[...] = ((zt - mean) * scale * cols[:, 2:3]).astype(BF16).astype(F32).T * ALPHA
 
@@ -512,13 +530,18 @@
 
     ret_at = unit(me)
 
-    def give_back(i, carry):
-        t = c * 16 + i
-        for k in range(2):
-            @pl.when(jnp.logical_or(t != me, c != k))
-            def _():
-                send(eo.at[k, unit(i)], ret.at[ret_at], rts.at[0], rtr.at[0], (t // NX, lax.rem(t, NX), y, k))
-        return carry
+    def give_back(h):
+        tx = c + 2 * h
+        for dz in far_z:
+            tz = lax.rem(z + dz, NZ)
+            for k in range(2):
+                def go():
+                    send(eo.at[k, unit(h * NZ + tz)], ret.at[ret_at], rts.at[0], rtr.at[0], (tz, tx, y, k))
+
+                if dz:
+                    go()
+                else:
+                    pl.when(jnp.logical_or(tx != x, c != k))(go)
 
     for h in (0, 1):
         for k in (0, 1):
@@ -528,11 +551,11 @@
                 wait(drecv.at[d, p, last], ddr.at[d, p, last])
                 value = value + drecv[d, p, last].astype(F32)
             eo[k, pl.ds(h * 128, 128), :] = value.astype(BF16)
-        lax.fori_loop(8 * h, 8 * h + 8, give_back, 0)
+        give_back(h)
 
     @pl.when(half == c)
     def _():
-        ret[ret_at, :] = eo[c, unit(lax.rem(me, 16)), :]
+        ret[ret_at, :] = eo[c, unit(place), :]
 
     wait_units(ret, rtr.at[0])
 
@@ -551,7 +574,8 @@
         s = 2 * dy + dc
         dev_id = (z, x, lax.rem(y + dy, NY), c if dc == 0 else other)
         send(stat2.at[0], stat2.at[s], s2s.at[s - 1], s2r.at[s - 1], dev_id)
-    for dy in far_first:
+    direct = (5, 3, 2, 6, 1, 7)
+    for dy in direct:
         send(fin.at[0], fin.at[2 * dy], fns.at[2 * dy - 1], fnr.at[2 * dy - 1], (z, x, lax.rem(y + dy, NY), c))
     for step in range(4):
         for d in range(2):
@@ -572,8 +596,10 @@
     for k, buf in enumerate((wg, wu, wd)):
         wait(buf.at[0], wsd.at[1 + k])
     wait(heads.at[0], hsd.at[0])
-    for r in range(7):
+    for r in (0, 1, 2, 4, 5, 6):
         wait(rsend.at[r], rsd.at[r])
+    for k in range(2):
+        wait(rsend.at[3, ends[k]], rsd.at[(3, 7)[k]])
     for s in range(15):
         wait(stat1.at[0], s1s.at[s])
     wait_units(disp, dps.at[0])
@@ -606,17 +632,19 @@
     finish(0, 0)
     wait(fin.at[1], fnr.at[0])
     finish(0, 1)
-    arrivals = far_first
+    arrivals = (*direct, 4)
     for i, dy in enumerate(arrivals):
         wait(fin.at[2 * dy], fnr.at[2 * dy - 1])
+        if dy == 5:
+            send(fin.at[10], fin.at[8], fns.at[7], fnr.at[7], (z, x, ym, c))
         send(fin.at[2 * dy], fin.at[2 * dy + 1], fns.at[2 * dy], fnr.at[2 * dy], partner)
         finish(dy, 0)
         if i:
             before_dy = arrivals[i - 1]
             wait(fin.at[2 * before_dy + 1], fnr.at[2 * before_dy])
             finish(before_dy, 1)
-    wait(fin.at[15], fnr.at[14])
-    finish(7, 1)
+    wait(fin.at[9], fnr.at[8])
+    finish(4, 1)
 
     for s in range(15):
         wait(stat2.at[0], s2s.at[s])
@@ -648,7 +676,7 @@
         fl(1, 2), pltpu.VMEM((2, 128), jnp.int32), fl(2, 128), fl(2, 128), fl(16, 128), fl(16, 128),
         bf(16, 128, 128), bf(32, 2048), bf(2, 2, 128, 256), bf(512, 128), bf(256, 128),
         dma((13,)), dma((2, 4, 5)), dma((8, 5)), dma((3, 2)), dma((3, 2)), dma((4,)), dma((4,)),
-        dma((3, 2)), dma((3, 2)), dma((3,)), dma((3,)), dma((1,)), dma((1,)), dma((7,)), dma((7,)),
+        dma((3, 2)), dma((3, 2)), dma((3,)), dma((3,)), dma((1,)), dma((1,)), dma((8,)), dma((8,)),
         dma((15,)), dma((15,)), dma((1,)), dma((1,)), dma((2, 4, 4)), dma((8, 4)),
         dma((2, 4, 4)), dma((2, 4, 4)), dma((1,)), dma((1,)), dma((15,)), dma((15,)), dma((15,)), dma((15,)),
         dma((6,)), pltpu.SemaphoreType.REGULAR((3,)), dma((16,)), dma((1,)), dma((1,)),

time: 105 us -> 103 us (0.981)
  Pallas kernels: 103 us -> 101 us
    pallas_call x1, Pallas kernels: 103 us -> 101 us  [on_device(): pl.pallas_call(kernel, out_shape=jax.ShapeDtypeStruct((128, 2048), BF16),...]
where the time goes in v5:
time: 103 us; the launch traced here: 102 us
  Pallas kernels  101 us (98%)
  local copies, waits for them, and re-layouts  1.88 us (2%)
    pallas_call x1, Pallas kernels, on_device(): pl.pallas_call(kernel, out_shape=jax.ShapeDtypeStruct((128, 2048), BF16),...  101 us

profile of v5, /device:TPU:1, one launch (start us, length us, event | category | flops | bytes accessed | tf_op | source)
XLA Modules:
  0.0 102.4 jit_solution(17889031618466383447)
XLA Ops:
  0.0 100.5 %layer.1 = bf16[128,2048]{1,0:T(8,128)(2,1)} custom-call(f32[1,2]{1,0:T(1,128)} %bitcast.9, s32[2,128]{1,0:T(2,128)} %bitcast.7, f32[2,128]{1,0:T(2,128)} %bitcast.8, f32[2,128]{1,0:T(2,128)} %hgain_in.1, f32[16,128]{1,0:T(8,128)} %bitcast.5, f32[16,128]{1,0:T(8,128)} %bitcast.6, bf16[128,2048]{1,0:T(8,128)(2,1)} %tok.1, bf16[128,128]{1,0:T(8,128)(2,1)} %qn.1, ...), custom_call_target="tpu_custom_call" | custom-call | tf_op jit(solution)/shard_map/layer/pallas_call | solution.py:684
  100.5 1.9 %copy.20 = bf16[128,2048]{1,0:T(8,128)(2,1)} copy(bf16[128,2048]{1,0:T(8,128)(2,1)} %layer.1) | data formatting | bytes 1048576

commit v6 on v5

--- a/solution.py
+++ b/solution.py
@@ -382,6 +382,55 @@
     def _():
         send(disp.at[unit(me)], xg.at[0, arrive_at], dps.at[0], dpr.at[0], partner)
 
+    def wait_units(ref, sem):
+        @pl.when(half == c)
+        def _():
+            wait(ref.at[pl.ds(0, 496)], sem)
+
+        @pl.when(half != c)
+        def _():
+            wait(ref, sem)
+
+    wait_units(xg.at[0], dpr.at[0])
+
+    def piece_of(h, k):
+        return pl.ds(k * 256 + h * 128, 128)
+
+    def xg_send(d, step, h, k, src_slot, dst_slot):
+        send(
+            xg.at[src_slot, piece_of(h, k)], xg.at[dst_slot, piece_of(h, k)], xgs.at[d, step, 2 * h + k],
+            xgr.at[dst_slot, 2 * h + k], (z, x, (yp, ym)[d], c),
+        )
+
+    def xg_wait(slot, h, k):
+        wait(xg.at[slot, piece_of(h, k)], xgr.at[slot, 2 * h + k])
+
+    def xg_arrive(d, h, k):
+        xg_wait(d, h, k)
+        if d < 3 or k == 0:
+            xg_send(0, d, h, k, d, d + 1)
+        xg_wait(4 + d, h, k)
+        if d < 3:
+            xg_send(1, d, h, k, 4 + d, 5 + d)
+        elif k == 1:
+            xg_send(1, d, h, k, 7, 4)
+
+    def slot_y(slot):
+        away = NY - slot if slot <= 4 else slot - 4
+        return lax.rem(y + away, NY)
+
+    def absorb(slot, h, start=False):
+        at = pl.ds(pl.multiple_of(slot_y(slot) * 256, 256), 256)
+        rows_in = jnp.concatenate([xg[slot, piece_of(h, 0), :], xg[slot, piece_of(h, 1), :]], axis=1)
+        for s in range(2):
+            for w, a in ((wg, accg), (wu, accu)):
+                value = dot(rows_in, w[s, at, :], 1, 0)
+                a[h, s] = value if start else a[h, s] + value
+
+    for h in (0, 1):
+        for k in (0, 1):
+            xg_send(0, 0, h, k, 0, 1)
+            xg_send(1, 0, h, k, 0, 5)
     for s in range(1, 16):
         wait(stat1.at[s], s1r.at[s - 1])
     total = functools.reduce(jnp.add, [stat1[s] for s in range(16)])
@@ -414,55 +463,6 @@
 
     mixed[...] = ((zt - mean) * scale * cols[:, 2:3]).astype(BF16).astype(F32).T * ALPHA
 
-    def wait_units(ref, sem):
-        @pl.when(half == c)
-        def _():
-            wait(ref.at[pl.ds(0, 496)], sem)
-
-        @pl.when(half != c)
-        def _():
-            wait(ref, sem)
-
-    wait_units(xg.at[0], dpr.at[0])
-
-    def piece_of(h, k):
-        return pl.ds(k * 256 + h * 128, 128)
-
-    def xg_send(d, step, h, k, src_slot, dst_slot):
-        send(
-            xg.at[src_slot, piece_of(h, k)], xg.at[dst_slot, piece_of(h, k)], xgs.at[d, step, 2 * h + k],
-            xgr.at[dst_slot, 2 * h + k], (z, x, (yp, ym)[d], c),
-        )
-
-    def xg_wait(slot, h, k):
-        wait(xg.at[slot, piece_of(h, k)], xgr.at[slot, 2 * h + k])
-
-    def xg_arrive(d, h, k):
-        xg_wait(d, h, k)
-        if d < 3 or k == 0:
-            xg_send(0, d, h, k, d, d + 1)
-        xg_wait(4 + d, h, k)
-        if d < 3:
-            xg_send(1, d, h, k, 4 + d, 5 + d)
-        elif k == 1:
-            xg_send(1, d, h, k, 7, 4)
-
-    def slot_y(slot):
-        away = NY - slot if slot <= 4 else slot - 4
-        return lax.rem(y + away, NY)
-
-    def absorb(slot, h, start=False):
-        at = pl.ds(pl.multiple_of(slot_y(slot) * 256, 256), 256)
-        rows_in = jnp.concatenate([xg[slot, piece_of(h, 0), :], xg[slot, piece_of(h, 1), :]], axis=1)
-        for s in range(2):
-            for w, a in ((wg, accg), (wu, accu)):
-                value = dot(rows_in, w[s, at, :], 1, 0)
-                a[h, s] = value if start else a[h, s] + value
-
-    for h in (0, 1):
-        for k in (0, 1):
-            xg_send(0, 0, h, k, 0, 1)
-            xg_send(1, 0, h, k, 0, 5)
     for h in (0, 1):
         absorb(0, h, True)
     for d in (1, 2, 3):
@@ -520,7 +520,8 @@
         pass_on(0, h, 1, 0)
         produce(h, 5)
         pass_on(1, h, 0, 0)
-        for r in (2, 6, 1, 7, 0):
+    for r in (2, 6, 1, 7, 0):
+        for h in (0, 1):
             produce(h, r)
     for step in (1, 2, 3):
         for h in (0, 1):

time: 103 us -> 103 us (level)
  no operation moved by 1% of the time
where the time goes in v6:
time: 103 us; the launch traced here: 102 us
  Pallas kernels  100 us (97%)
  local copies, waits for them, and re-layouts  1.88 us (2%)
    pallas_call x1, Pallas kernels, on_device(): pl.pallas_call(kernel, out_shape=jax.ShapeDtypeStruct((128, 2048), BF16),...  100 us

profile of v6, /device:TPU:1, one launch (start us, length us, event | category | flops | bytes accessed | tf_op | source)
XLA Modules:
  0.0 102.4 jit_solution(3893711547500450496)
XLA Ops:
  0.0 100.5 %layer.1 = bf16[128,2048]{1,0:T(8,128)(2,1)} custom-call(f32[1,2]{1,0:T(1,128)} %bitcast.9, s32[2,128]{1,0:T(2,128)} %bitcast.7, f32[2,128]{1,0:T(2,128)} %bitcast.8, f32[2,128]{1,0:T(2,128)} %hgain_in.1, f32[16,128]{1,0:T(8,128)} %bitcast.5, f32[16,128]{1,0:T(8,128)} %bitcast.6, bf16[128,2048]{1,0:T(8,128)(2,1)} %tok.1, bf16[128,128]{1,0:T(8,128)(2,1)} %qn.1, ...), custom_call_target="tpu_custom_call" | custom-call | tf_op jit(solution)/shard_map/layer/pallas_call | solution.py:685
  100.5 1.9 %copy.20 = bf16[128,2048]{1,0:T(8,128)(2,1)} copy(bf16[128,2048]{1,0:T(8,128)(2,1)} %layer.1) | data formatting | bytes 1048576
